TPU v7x, 32 devices: a whole 2x2x4 slice. The times are simulated.
32 devices in a mesh: sp: 4 (over z), fs: 4 (over y, x), tp: 2 (over core).
Axes of the slice: x: 2, y: 2, z: 4, core: 2. Of those that a mesh axis runs over, the one named last changes fastest.
Arguments:
- tokens: bfloat16 [4, 1024, 2048], P('fs', ('sp', 'tp')), may hold values from -6 to 6
- query_weight: bfloat16 [2048, 2048], P(('sp', 'fs'), 'tp'), may hold values from -0.125 to 0.125
- forget_weight: bfloat16 [2048, 2048], P(('sp', 'fs'), 'tp'), may hold values from -0.125 to 0.125
- value_weight: bfloat16 [2048, 2048], P(('sp', 'fs'), 'tp'), may hold values from -0.125 to 0.125
- convolution_gate_weight: bfloat16 [2048, 1024], P(('sp', 'fs'), 'tp'), may hold values from -0.125 to 0.125
- convolution_multiplier_weight: bfloat16 [2048, 1024], P(('sp', 'fs'), 'tp'), may hold values from -0.125 to 0.125
- convolution_input_weight: bfloat16 [2048, 1024], P(('sp', 'fs'), 'tp'), may hold values from -0.125 to 0.125
- gate_headroom: float32 [2048], P('tp'), may hold values from 9.765625e-05 to 0.06
- added_log_rate: float32 [4, 16, 1024], P('fs', 'tp', 'sp'), may hold values from -1.6 to 0
- initial_state: float32 [4, 16, 128, 128], P('fs', 'tp'), may hold values from -0.5 to 0.5
- head_norm_gain: float32 [2048], P('tp'), may hold values from 0.1 to 1.9
- convolution_taps: float32 [3, 1024], P(None, 'tp'), may hold values from -3.5 to 3.5
- convolution_bias: float32 [1024], P('tp'), may hold values from -4 to 4
- recurrence_output_weight: bfloat16 [2048, 2048], P('tp', ('sp', 'fs')), may hold values from -0.109375 to 0.109375
- convolution_output_weight: bfloat16 [1024, 2048], P('tp', ('sp', 'fs')), may hold values from -0.109375 to 0.109375
Outputs:
- mixed: bfloat16 [4, 1024, 2048], P('fs', ('sp', 'tp'))
All inputs are finite; a program needn't handle non-finite values.
Results may differ from a plain program's by a relative error of at most 0.018.
Values may be sent and summed in bfloat16 or wider, within the bound.
A program may use at most 64 MiB of HBM per device.

v0:
```python
import functools

import jax
import jax.numpy as jnp
from jax import lax
from jax.experimental import pallas as pl
from jax.experimental.pallas import tpu as pltpu
from jax.sharding import PartitionSpec as P

DK = 128
KW = 3
BLOCK_POSITIONS = 64


def carried_in(part, axis, combine, identity):
    place = lax.axis_index(axis)
    gathered = jax.tree.map(lambda a: lax.all_gather(a, axis), part)
    state = jax.tree.map(lambda a, e: jnp.zeros_like(a) + jnp.asarray(e, a.dtype), part, identity)

    def one(hop, state):
        return combine(
            state, jax.tree.map(lambda a: lax.dynamic_index_in_dim(a, hop, 0, False), gathered)
        )

    return lax.fori_loop(0, place, one, state)


def from_behind(block, axis, distance):
    devices = range(lax.axis_size(axis))
    route = [(i - distance, i) for i in devices if i - distance in devices]
    return lax.ppermute(block, axis, route)


def to_blocks(values, number_of_heads):
    number_of_blocks = values.shape[0] // BLOCK_POSITIONS
    return jnp.transpose(
        values.reshape(number_of_blocks, BLOCK_POSITIONS, number_of_heads, DK), (2, 0, 1, 3)
    )


def within_block_recurrence(
    query_vectors, forget_logits, value_vectors, gate_headroom, extra_rates
):
    number_of_heads = extra_rates.shape[0]
    number_of_blocks = query_vectors.shape[0] // BLOCK_POSITIONS
    query_scaled = to_blocks(query_vectors.astype(jnp.float32), number_of_heads) * DK ** (-0.5)
    gated_key = to_blocks(
        gate_headroom[None, :] * jax.nn.sigmoid(-forget_logits.astype(jnp.float32)), number_of_heads
    )
    forget_log_rate = (
        jnp.log1p(-gated_key)
        + extra_rates.reshape(number_of_heads, number_of_blocks, BLOCK_POSITIONS)[..., None]
    )
    values = to_blocks(value_vectors.astype(jnp.float32), number_of_heads)
    cumulative = jnp.cumsum(forget_log_rate, axis=2)
    query_decayed = query_scaled * jnp.exp(cumulative)
    key_decayed = gated_key * jnp.exp(-cumulative)
    scores = jnp.einsum(
        "hnik,hnjk->hnij", query_decayed, key_decayed, precision=lax.Precision.HIGHEST
    )
    causal = jnp.tril(jnp.ones((BLOCK_POSITIONS, BLOCK_POSITIONS), dtype=bool))
    scores = jnp.where(causal, scores, 0.0)
    within = jnp.einsum("hnij,hnjv->hniv", scores, values, precision=lax.Precision.HIGHEST)
    final_log = cumulative[:, :, -1, :]
    contrib = jnp.einsum(
        "hnck,hncv->hnkv",
        gated_key * jnp.exp(final_log[:, :, None, :] - cumulative),
        values,
        precision=lax.Precision.HIGHEST,
    )
    decays = jnp.exp(final_log)

    def advance(current, block_pair):
        return (block_pair[0][..., None] * current + block_pair[1], current)

    empty_state = jnp.zeros((number_of_heads, DK, DK), jnp.float32)
    local_total, entering = lax.scan(
        advance, empty_state, (jnp.moveaxis(decays, 1, 0), jnp.moveaxis(contrib, 1, 0))
    )
    entering = jnp.moveaxis(entering, 0, 1)
    before = jnp.exp(jnp.cumsum(final_log, axis=1) - final_log)
    device_decay = jnp.exp(jnp.sum(final_log, axis=1))
    return (query_decayed, within, entering, before, device_decay, local_total)


def finish(query_decayed, within, entering, before, carried, head_norm_gain):
    number_of_heads = query_decayed.shape[0]
    states = entering + before[..., None] * carried[:, None]
    carried_term = jnp.einsum(
        "hnck,hnkv->hncv", query_decayed, states, precision=lax.Precision.HIGHEST
    )
    length = query_decayed.shape[1] * BLOCK_POSITIONS
    recurrence_unnormed = jnp.transpose(within + carried_term, (1, 2, 0, 3)).reshape(
        length, number_of_heads, DK
    )
    mean_square = jnp.mean(recurrence_unnormed * recurrence_unnormed, axis=-1, keepdims=True)
    rec_out = (
        recurrence_unnormed
        * lax.rsqrt(mean_square + 1e-06)
        * head_norm_gain.reshape(number_of_heads, DK)
    )
    return rec_out.reshape(length, number_of_heads * DK).astype(jnp.bfloat16)


def chain_combine(earlier_part, later_part):
    return (
        earlier_part[0] * later_part[0],
        later_part[0][..., None] * earlier_part[1] + later_part[1],
    )


def shards(
    tokens,
    query_weight,
    forget_weight,
    value_weight,
    convolution_gate_weight,
    convolution_multiplier_weight,
    convolution_input_weight,
    gate_headroom,
    added_log_rate,
    initial_state,
    head_norm_gain,
    convolution_taps,
    convolution_bias,
    recurrence_output_weight,
    convolution_output_weight,
):
    own_rows = tokens[0]
    gathered = (
        lax.all_gather(query_weight, ("sp", "fs"), axis=0, tiled=True),
        lax.all_gather(forget_weight, ("sp", "fs"), axis=0, tiled=True),
        lax.all_gather(value_weight, ("sp", "fs"), axis=0, tiled=True),
        lax.all_gather(convolution_gate_weight, ("sp", "fs"), axis=0, tiled=True),
        lax.all_gather(convolution_multiplier_weight, ("sp", "fs"), axis=0, tiled=True),
        lax.all_gather(convolution_input_weight, ("sp", "fs"), axis=0, tiled=True),
        lax.all_gather(recurrence_output_weight, ("sp", "fs"), axis=1, tiled=True),
        lax.all_gather(convolution_output_weight, ("sp", "fs"), axis=1, tiled=True),
    )
    in_weights = gathered[:6]
    out_rec = gathered[6]
    out_conv = gathered[7]
    block_rows = lax.all_gather(own_rows, "tp", axis=0, tiled=True)
    projected = jnp.concatenate(
        [
            jnp.dot(block_rows, weight, preferred_element_type=jnp.float32).astype(jnp.bfloat16)
            for weight in in_weights
        ],
        axis=1,
    )
    rec_width = query_weight.shape[1]
    conv_width = convolution_gate_weight.shape[1]
    query_vectors = projected[:, :rec_width]
    forget_logits = projected[:, rec_width : 2 * rec_width]
    value_vectors = projected[:, 2 * rec_width : 3 * rec_width]
    conv_base = 3 * rec_width
    conv_gate = projected[:, conv_base : conv_base + conv_width]
    conv_mult = projected[:, conv_base + conv_width : conv_base + 2 * conv_width]
    conv_input = projected[:, conv_base + 2 * conv_width : conv_base + 3 * conv_width]
    query_decayed, within, entering, before, device_decay, local_total = within_block_recurrence(
        query_vectors, forget_logits, value_vectors, gate_headroom, added_log_rate[0]
    )
    conv_prod = conv_mult.astype(jnp.float32) * conv_input.astype(jnp.float32)
    length = conv_prod.shape[0]
    tail_rows = conv_prod[length - (KW - 1) :]
    unit_decay = jnp.ones_like(device_decay)
    empty_state = jnp.zeros_like(local_total)
    prior_decay, prior_state = carried_in(
        (device_decay, local_total), "sp", chain_combine, (unit_decay, empty_state)
    )
    prior_rows = from_behind(tail_rows, "sp", 1)
    carried = prior_decay[..., None] * initial_state[0] + prior_state
    rec_out = finish(query_decayed, within, entering, before, carried, head_norm_gain)
    extended = jnp.concatenate([prior_rows, conv_prod], axis=0)
    conv_y = jnp.broadcast_to(convolution_bias[None, :], conv_prod.shape)
    for j in range(KW):
        conv_y = conv_y + convolution_taps[j][None, :] * extended[j : j + length]
    conv_out = (conv_gate.astype(jnp.float32) * conv_y).astype(jnp.bfloat16)
    mixed = lax.psum_scatter(
        (
            jnp.dot(rec_out, out_rec, preferred_element_type=jnp.float32)
            + jnp.dot(conv_out, out_conv, preferred_element_type=jnp.float32)
        ).astype(jnp.bfloat16),
        "tp",
        scatter_dimension=0,
        tiled=True,
    )
    return mixed[None]


MESH = pl.DeviceIdType.MESH
F32 = jnp.float32
BF16 = jnp.bfloat16
CONTRACT_LAST = (((1,), (1,)), ((), ()))
CONTRACT_FIRST = (((0,), (0,)), ((), ()))


def layer_kernel(
    n_sp, n_fs, tok, wq, wf, wv, cg, cm, ci, ro, co, headroom, rate, init, gain, taps, bias,
    out, tokens, win, wout, rates, state, ext, sib_send, sib_recv, mine, z_send, z_recv,
    loc_sem, send_sem, win_z, wout_z, win_f, wout_f, tok_z, tok_t, rate_z, sib_sem, zr_sem,
    rs_send,
):
    sp, fs, tp = lax.axis_index("sp"), lax.axis_index("fs"), lax.axis_index("tp")
    other = 1 - tp
    rows = wq.shape[0]
    rec = wq.shape[1] // n_sp
    con = cg.shape[1] // n_sp
    span = tok.shape[0]
    heads = rec // DK
    wide = tok.shape[1]

    def peer(**where):
        return {"sp": where.get("sp", sp), "fs": where.get("fs", fs), "tp": where.get("tp", tp)}

    def z_at(d):
        return lax.rem(sp + d, n_sp)

    def f_at(e):
        return lax.rem(fs + e, n_fs)

    parts = []
    at = 0
    for ref, width in ((wq, rec), (wf, rec), (wv, rec), (cg, con), (cm, con), (ci, con)):
        parts.append((ref, at, width))
        at += width

    def in_slot(s, f):
        return win.at[pl.ds(pl.multiple_of((s * n_fs + f) * rows, rows), rows)]

    def in_piece(s, f, at, width):
        first = pl.multiple_of((s * n_fs + f) * rows, rows)
        return win.at[pl.ds(first, rows), pl.ds(at, width)]

    def out_slot(s, f):
        lanes = ro.shape[1]
        return wout.at[:, pl.ds(pl.multiple_of((s * n_fs + f) * lanes, lanes), lanes)]

    def out_piece(s, f, at, width):
        lanes = ro.shape[1]
        first = pl.multiple_of((s * n_fs + f) * lanes, lanes)
        return wout.at[pl.ds(at, width), pl.ds(first, lanes)]

    def weight_sources(s):
        ins = [
            (ref.at[:, pl.ds(pl.multiple_of(s * width, width), width)], at, width)
            for ref, at, width in parts
        ]
        outs = [
            (ro.at[pl.ds(pl.multiple_of(s * rec, rec), rec)], 0, rec),
            (co.at[pl.ds(pl.multiple_of(s * con, con), con)], rec, con),
        ]
        return ins, outs

    local = []
    ins, outs = weight_sources(sp)
    for ref, at, width in ins:
        local.append((ref, in_piece(sp, fs, at, width)))
    for ref, at, width in outs:
        local.append((ref, out_piece(sp, fs, at, width)))
    local.append((tok, tokens.at[sp * 2 + tp]))
    local.append((rate.at[sp], rates.at[sp]))
    local = [pltpu.make_async_copy(*pair, loc_sem.at[i]) for i, pair in enumerate(local)]
    for copy in local:
        copy.start()

    barrier = pltpu.get_barrier_semaphore()
    for d in range(1, n_sp):
        pl.semaphore_signal(barrier, inc=1, device_id=peer(sp=z_at(d)), device_id_type=MESH)
    for e in range(1, n_fs):
        pl.semaphore_signal(barrier, inc=1, device_id=peer(fs=f_at(e)), device_id_type=MESH)
    pl.semaphore_signal(barrier, inc=1, device_id=peer(tp=other), device_id_type=MESH)
    pl.semaphore_wait(barrier, n_sp + n_fs - 1)

    sent = []

    def remote(src, dst, recv, to, start=True):
        copy = pltpu.make_async_remote_copy(
            src_ref=src, dst_ref=dst, send_sem=send_sem.at[len(sent) if start else 0], recv_sem=recv, device_id=to,
            device_id_type=MESH,
        )
        if start:
            copy.start()
            sent.append(copy)
        return copy

    near = sorted(range(1, n_sp), key=lambda d: min(d, n_sp - d))
    for d in near:
        to = peer(sp=z_at(d))
        ins, outs = weight_sources(z_at(d))
        for i, (ref, at, width) in enumerate(ins):
            remote(ref, in_piece(sp, fs, at, width), win_z.at[d, i], to)
        for i, (ref, at, width) in enumerate(outs):
            remote(ref, out_piece(sp, fs, at, width), wout_z.at[d, i], to)
        remote(tok, tokens.at[sp * 2 + tp], tok_z.at[d], to)
        remote(rate.at[z_at(d)], rates.at[sp], rate_z.at[d], to)
    remote(tok, tokens.at[sp * 2 + tp], tok_t.at[0], peer(tp=other))

    for copy in local:
        copy.wait()

    def spread(d):
        s = z_at(n_sp - d)
        for e in range(1, n_fs):
            remote(in_slot(s, fs), in_slot(s, fs), win_f.at[e, d], peer(fs=f_at(e)))
        for e in range(1, n_fs):
            remote(out_slot(s, fs), out_slot(s, fs), wout_f.at[e, d], peer(fs=f_at(e)))

    spread(0)
    for d in near:
        s = z_at(n_sp - d)
        me = peer(tp=other)
        for i, (ref, at, width) in enumerate(parts):
            piece = in_piece(s, fs, at, width)
            remote(piece, piece, win_z.at[d, i], me, start=False).wait_recv()
        for i, (at, width) in enumerate(((0, rec), (rec, con))):
            piece = out_piece(s, fs, at, width)
            remote(piece, piece, wout_z.at[d, i], me, start=False).wait_recv()
        spread(d)
        piece = tokens.at[s * 2 + tp]
        remote(piece, piece, tok_z.at[d], me, start=False).wait_recv()
        remote(piece, piece, tok_t.at[d], me)
        remote(rates.at[s], rates.at[s], rate_z.at[d], me, start=False).wait_recv()
    for d in range(n_sp):
        s = z_at((n_sp - d) % n_sp)
        piece = tokens.at[s * 2 + other]
        remote(piece, piece, tok_t.at[d], peer(tp=other), start=False).wait_recv()
    for d in range(n_sp):
        s = z_at((n_sp - d) % n_sp)
        for e in range(1, n_fs):
            f = f_at(n_fs - e)
            remote(in_slot(s, f), in_slot(s, f), win_f.at[e, d], peer(tp=other), start=False).wait_recv()
            remote(out_slot(s, f), out_slot(s, f), wout_f.at[e, d], peer(tp=other), start=False).wait_recv()
    for copy in sent:
        copy.wait_send()

    for h in range(heads):
        state[h] = init[sp * heads + h].T
    ext[0:8] = jnp.zeros((8, con), F32)
    lane_rec = pl.ds(pl.multiple_of(sp * rec, rec), rec)
    lane_con = pl.ds(pl.multiple_of(sp * con, con), con)
    row_id = lax.broadcasted_iota(jnp.int32, (span, span), 0)
    col_id = lax.broadcasted_iota(jnp.int32, (span, span), 1)
    causal = row_id >= col_id
    lower = causal.astype(F32)
    upper = (row_id <= col_id).astype(F32)
    length = 2 * span

    def sib_copy(s):
        return pltpu.make_async_remote_copy(
            src_ref=sib_send.at[s], dst_ref=sib_recv.at[s], send_sem=rs_send.at[0, s],
            recv_sem=sib_sem.at[s], device_id=peer(tp=other), device_id_type=MESH,
        )

    def z_copy(s):
        d = lax.rem(s - sp + n_sp, n_sp)
        return pltpu.make_async_remote_copy(
            src_ref=z_send.at[s], dst_ref=z_recv.at[d], send_sem=rs_send.at[1, d],
            recv_sem=zr_sem.at[d], device_id=peer(sp=s), device_id_type=MESH,
        )

    def pass_on(s):
        sib_copy(s).wait_recv()
        total = mine[s] + sib_recv[s].astype(F32)

        @pl.when(s != sp)
        def _():
            z_send[s] = total.astype(BF16)
            z_copy(s).start()

        @pl.when(s == sp)
        def _():
            z_recv[0] = total.astype(BF16)

    def step(s, carry):
        block = jnp.concatenate([tokens[2 * s], tokens[2 * s + 1]], axis=0)

        def project(at, width):
            return jnp.dot(
                block, win[:, pl.ds(at, width)], preferred_element_type=F32
            ).astype(BF16)

        query = project(0, rec).astype(F32) * DK ** (-0.5)
        forget = project(rec, rec).astype(F32)
        value = project(2 * rec, rec)
        base = 3 * rec
        conv_gate = project(base, con).astype(F32)
        prod = project(base + con, con).astype(F32) * project(base + 2 * con, con).astype(F32)
        key_gate = headroom[:, lane_rec] * jax.nn.sigmoid(-forget)
        log_forget = jnp.log1p(-key_gate)
        gains = gain[:, lane_rec]
        halves = []
        for c in range(2):
            part = slice(c * span, (c + 1) * span)
            cum = jnp.dot(lower, log_forget[part], precision=lax.Precision.HIGHEST)
            extra = jnp.dot(rates[s][:, part], upper, precision=lax.Precision.HIGHEST)
            extra_t = extra.T
            grow = jnp.exp(cum)
            query_grow = query[part] * grow
            key_grow = (key_gate[part] / grow).astype(BF16)
            last = cum[span - 1 :, :]
            key_last = key_gate[part] * jnp.exp(last - cum)
            last_decay = jnp.exp(last)
            pieces = []
            for h in range(heads):
                lanes = slice(h * DK, (h + 1) * DK)
                row = extra[h : h + 1]
                column = extra_t[:, h : h + 1]
                end = row[:, span - 1 :]
                scores = lax.dot_general(
                    query_grow[:, lanes].astype(BF16), key_grow[:, lanes], CONTRACT_LAST,
                    preferred_element_type=F32,
                )
                decay = jnp.exp(jnp.where(causal, column - row, 0.0))
                scores = jnp.where(causal, scores * decay, 0.0).astype(BF16)
                values = value[part, lanes]
                before = state[h]
                raw = jnp.dot(scores, values, preferred_element_type=F32)
                raw = raw + lax.dot_general(
                    (query_grow[:, lanes] * jnp.exp(column)).astype(BF16), before.astype(BF16),
                    CONTRACT_LAST, preferred_element_type=F32,
                )
                keys = (key_last[:, lanes] * jnp.exp(end - column)).astype(BF16)
                state[h] = before * (last_decay[:, lanes] * jnp.exp(end)) + lax.dot_general(
                    values, keys, CONTRACT_FIRST, preferred_element_type=F32
                )
                square = jnp.mean(raw * raw, axis=-1, keepdims=True)
                pieces.append((raw * lax.rsqrt(square + 1e-06) * gains[:, lanes]).astype(BF16))
            halves.append(jnp.concatenate(pieces, axis=1))
        ext[8:] = prod
        conv = jnp.broadcast_to(bias[:, lane_con], prod.shape)
        for j in range(KW):
            conv = conv + taps[j : j + 1, lane_con] * ext[pl.ds(8 - (KW - 1) + j, length)]
        ext[0:8] = ext[length:]
        conv_out = (conv_gate * conv).astype(BF16)
        both = jnp.concatenate([jnp.concatenate(halves, axis=0), conv_out], axis=1)
        chunk = min(512, wide)
        for n in range(0, wide, chunk):
            partial = jnp.dot(both, wout[:, n : n + chunk], preferred_element_type=F32)
            first = partial[:span]
            second = partial[span:]
            mine[s, :, n : n + chunk] = jnp.where(tp == 0, first, second)
            sib_send[s, :, n : n + chunk] = jnp.where(tp == 0, second, first).astype(BF16)
        sib_copy(s).start()

        @pl.when(s > 0)
        def _():
            pass_on(s - 1)

        return carry

    lax.fori_loop(0, n_sp, step, 0)
    pass_on(n_sp - 1)
    for d in range(1, n_sp):
        pltpu.make_async_remote_copy(
            src_ref=z_recv.at[d], dst_ref=z_recv.at[d], send_sem=rs_send.at[1, d],
            recv_sem=zr_sem.at[d], device_id=peer(tp=other), device_id_type=MESH,
        ).wait_recv()
    total = z_recv[0].astype(F32)
    for d in range(1, n_sp):
        total = total + z_recv[d].astype(F32)
    out[...] = total.astype(BF16)
    for s in range(n_sp):
        sib_copy(s).wait_send()
    for d in range(1, n_sp):
        pltpu.make_async_remote_copy(
            src_ref=z_send.at[z_at(d)], dst_ref=z_recv.at[d], send_sem=rs_send.at[1, d],
            recv_sem=zr_sem.at[d], device_id=peer(sp=z_at(d)), device_id_type=MESH,
        ).wait_send()


def sequence_shards(n_sp, n_fs, *arrays):
    (tok, wq, wf, wv, cg, cm, ci, headroom, rate, init, gain, taps, bias, ro, co) = arrays
    span, wide = tok.shape[1:]
    rec, con = wq.shape[1] // n_sp, cg.shape[1] // n_sp
    heads = rec // DK
    by_place = rate[0].reshape(n_sp, heads, rate.shape[2])
    by_place = jnp.pad(by_place, ((0, 0), (0, 8 - heads), (0, 0)))
    hbm = pl.BlockSpec(memory_space=pl.ANY)
    vmem = pl.BlockSpec(memory_space=pltpu.VMEM)
    dma = pltpu.SemaphoreType.DMA
    mixed = pl.pallas_call(
        functools.partial(layer_kernel, n_sp, n_fs),
        out_shape=jax.ShapeDtypeStruct((span, wide), BF16),
        in_specs=[hbm] * 9 + [vmem, hbm] + [vmem] * 4,
        out_specs=vmem,
        scratch_shapes=[
            pltpu.VMEM((2 * n_sp, span, wide), BF16),
            pltpu.VMEM((wide, 3 * (rec + con)), BF16),
            pltpu.VMEM((rec + con, wide), BF16),
            pltpu.VMEM((n_sp, 8, rate.shape[2]), F32),
            pltpu.VMEM((heads, DK, DK), F32),
            pltpu.VMEM((8 + 2 * span, con), F32),
            pltpu.VMEM((n_sp, span, wide), BF16),
            pltpu.VMEM((n_sp, span, wide), BF16),
            pltpu.VMEM((n_sp, span, wide), F32),
            pltpu.VMEM((n_sp, span, wide), BF16),
            pltpu.VMEM((n_sp, span, wide), BF16),
            dma((10,)),
            dma(((n_sp - 1) * 10 + n_sp * (1 + 2 * (n_fs - 1)),)),
            dma((n_sp, 6)),
            dma((n_sp, 2)),
            dma((n_fs, n_sp)),
            dma((n_fs, n_sp)),
            dma((n_sp,)),
            dma((n_sp,)),
            dma((n_sp,)),
            dma((n_sp,)),
            dma((n_sp,)),
            dma((2, n_sp)),
        ],
        compiler_params=pltpu.CompilerParams(
            collective_id=0, has_side_effects=True, vmem_limit_bytes=60 * 2**20
        ),
    )(
        tok[0], wq, wf, wv, cg, cm, ci, ro, co, headroom[None], by_place, init[0], gain[None],
        taps, bias[None],
    )
    return mixed[None]


def choose_plan(sizes, *arrays):
    n_sp, n_fs = sizes["sp"], sizes["fs"]
    rows, rec = arrays[1].shape
    con = arrays[4].shape[1]
    span = arrays[0].shape[1]
    even = (
        sizes["tp"] == 2
        and arrays[0].shape[0] == 1
        and rec % (n_sp * DK) == 0
        and rec // (n_sp * DK) <= 8
        and con % (n_sp * 128) == 0
        and rows % 128 == 0
        and span == DK
        and arrays[13].shape[1] % 128 == 0
    )
    return sequence_shards(n_sp, n_fs, *arrays) if even else shards(*arrays)


def solution(mesh):
    in_specs = (
        P("fs", ("sp", "tp"), None),
        P(("sp", "fs"), "tp"),
        P(("sp", "fs"), "tp"),
        P(("sp", "fs"), "tp"),
        P(("sp", "fs"), "tp"),
        P(("sp", "fs"), "tp"),
        P(("sp", "fs"), "tp"),
        P("tp"),
        P("fs", "tp", "sp"),
        P("fs", "tp", None, None),
        P("tp"),
        P(None, "tp"),
        P("tp"),
        P("tp", ("sp", "fs")),
        P("tp", ("sp", "fs")),
    )
    out_specs = P("fs", ("sp", "tp"), None)
    body = functools.partial(choose_plan, dict(mesh.shape))
    return jax.shard_map(body, mesh=mesh, in_specs=in_specs, out_specs=out_specs, check_vma=False)
```

profile of v0, /device:TPU:28, one launch (start us, length us, event | category | flops | bytes accessed | tf_op | source)
XLA Modules:
  0.0 150.1 jit_solution(13416257417172974741)
XLA Ops:
  0.0 0.0 copy-start
  0.0 0.7 copy-done
  0.7 0.6 pad.4.rate
  1.3 146.9 %shard_map.145 = bf16[128,2048]{1,0:T(8,128)(2,1)} custom-call(bf16[128,2048]{1,0:T(8,128)(2,1)} %bitcast.7, bf16[128,1024]{1,0:T(8,128)(2,1)} %wq.1, bf16[128,1024]{1,0:T(8,128)(2,1)} %wf.1, bf16[128,1024]{1,0:T(8,128)(2,1)} %wv.1, bf16[128,512]{1,0:T(8,128)(2,1)} %cg.1, bf16[128,512]{1,0:T(8,128)(2,1)} %cm.1, bf16[128,512]{1,0:T(8,128)(2,1)} %ci.1, ...), custom_call_target="tpu_custom_call" | custom-call | tf_op jit(solution)/shard_map/pallas_call | solution.py:482
  148.2 1.9 %copy.17 = bf16[1,128,2048]{2,1,0:T(8,128)(2,1)} copy(bf16[1,128,2048]{2,1,0:T(8,128)(2,1)} %bitcast.6) | data formatting | bytes 1048576
  (1 shorter events, 0.0 us)
Async XLA Ops:
  0.0 0.7 copy-start
where the time goes:
time: 150 us
  Pallas kernels  147 us (98%)
  local copies, waits for them, and re-layouts  3.21 us (2%)
    pallas_call x1, Pallas kernels, sequence_shards(): pl.pallas_call(functools.partial(layer_kernel, n_sp, n_fs), out_shape=jax...  147 us

commit v1 on v0

--- a/solution.py
+++ b/solution.py
@@ -193,13 +193,15 @@
 BF16 = jnp.bfloat16
 CONTRACT_LAST = (((1,), (1,)), ((), ()))
 CONTRACT_FIRST = (((0,), (0,)), ((), ()))
+TOKEN_PIECES = 4
+OUT_PIECES = 4
 
 
 def layer_kernel(
-    n_sp, n_fs, tok, wq, wf, wv, cg, cm, ci, ro, co, headroom, rate, init, gain, taps, bias,
-    out, tokens, win, wout, rates, state, ext, sib_send, sib_recv, mine, z_send, z_recv,
-    loc_sem, send_sem, win_z, wout_z, win_f, wout_f, tok_z, tok_t, rate_z, sib_sem, zr_sem,
-    rs_send,
+    n_sp, n_fs, tok, wq, wf, wv, cg, cm, ci, ro, co, rate, init, headroom, gain, taps, bias,
+    out, tokens, win, wout, rates, first_state, state, ext, both, sib_send, sib_recv, mine, z_send,
+    z_recv, rl_recv, loc_sem, send_sem, win_z, wout_z, win_f, wout_f, tok_z, tok_t, rate_z, up_send,
+    down_send, own_send, tok_t_send, sib_sem, sib_out, zr_sem, rl_sem, rs_send,
 ):
     sp, fs, tp = lax.axis_index("sp"), lax.axis_index("fs"), lax.axis_index("tp")
     other = 1 - tp
@@ -209,15 +211,31 @@
     span = tok.shape[0]
     heads = rec // DK
     wide = tok.shape[1]
+    lanes_out = ro.shape[1]
+    chunks, chunk = mine.shape[1], mine.shape[3]
+    sub = span // TOKEN_PIECES
 
     def peer(**where):
         return {"sp": where.get("sp", sp), "fs": where.get("fs", fs), "tp": where.get("tp", tp)}
 
-    def z_at(d):
-        return lax.rem(sp + d, n_sp)
-
-    def f_at(e):
-        return lax.rem(fs + e, n_fs)
+    def z_at(k):
+        place, bit = sp, 1
+        while bit < n_sp:
+            if k & bit:
+                place = place + bit * (1 - 2 * lax.rem(sp // bit, 2))
+            bit *= 2
+        return place
+
+    half_ring = n_fs // 2
+
+    def ring(p):
+        return p + (p // half_ring) * (3 * half_ring - 1 - 2 * p)
+
+    at_ring = ring(fs)
+    left = ring(lax.rem(at_ring + n_fs - 1, n_fs))
+    right = ring(lax.rem(at_ring + 1, n_fs))
+    across = ring(lax.rem(at_ring + 2, n_fs))
+    sibling = peer(tp=other)
 
     parts = []
     at = 0
@@ -225,117 +243,232 @@
         parts.append((ref, at, width))
         at += width
 
-    def in_slot(s, f):
-        return win.at[pl.ds(pl.multiple_of((s * n_fs + f) * rows, rows), rows)]
+    def in_rows(s, f, first, count):
+        return win.at[pl.ds(pl.multiple_of((s * n_fs + f) * rows + first, count), count)]
 
     def in_piece(s, f, at, width):
         first = pl.multiple_of((s * n_fs + f) * rows, rows)
         return win.at[pl.ds(first, rows), pl.ds(at, width)]
 
-    def out_slot(s, f):
-        lanes = ro.shape[1]
-        return wout.at[:, pl.ds(pl.multiple_of((s * n_fs + f) * lanes, lanes), lanes)]
-
     def out_piece(s, f, at, width):
-        lanes = ro.shape[1]
-        first = pl.multiple_of((s * n_fs + f) * lanes, lanes)
-        return wout.at[pl.ds(at, width), pl.ds(first, lanes)]
-
-    def weight_sources(s):
-        ins = [
+        first = pl.multiple_of((s * n_fs + f) * lanes_out, lanes_out)
+        return wout.at[pl.ds(at, width), pl.ds(first, lanes_out)]
+
+    def in_sources(s):
+        return [
             (ref.at[:, pl.ds(pl.multiple_of(s * width, width), width)], at, width)
             for ref, at, width in parts
         ]
-        outs = [
+
+    def out_sources(s):
+        return [
             (ro.at[pl.ds(pl.multiple_of(s * rec, rec), rec)], 0, rec),
             (co.at[pl.ds(pl.multiple_of(s * con, con), con)], rec, con),
         ]
-        return ins, outs
-
-    local = []
-    ins, outs = weight_sources(sp)
-    for ref, at, width in ins:
-        local.append((ref, in_piece(sp, fs, at, width)))
-    for ref, at, width in outs:
-        local.append((ref, out_piece(sp, fs, at, width)))
+
+    local = [(ref, in_piece(sp, fs, at, width)) for ref, at, width in in_sources(sp)]
+    local += [(ref, out_piece(sp, fs, at, width)) for ref, at, width in out_sources(sp)]
     local.append((tok, tokens.at[sp * 2 + tp]))
-    local.append((rate.at[sp], rates.at[sp]))
+    local.append((rate, rates.at[sp]))
+    local.append((init.at[pl.ds(sp * heads, heads)], first_state))
     local = [pltpu.make_async_copy(*pair, loc_sem.at[i]) for i, pair in enumerate(local)]
     for copy in local:
         copy.start()
 
     barrier = pltpu.get_barrier_semaphore()
-    for d in range(1, n_sp):
-        pl.semaphore_signal(barrier, inc=1, device_id=peer(sp=z_at(d)), device_id_type=MESH)
-    for e in range(1, n_fs):
-        pl.semaphore_signal(barrier, inc=1, device_id=peer(fs=f_at(e)), device_id_type=MESH)
-    pl.semaphore_signal(barrier, inc=1, device_id=peer(tp=other), device_id_type=MESH)
-    pl.semaphore_wait(barrier, n_sp + n_fs - 1)
+    for k in range(1, n_sp):
+        pl.semaphore_signal(barrier, inc=1, device_id=peer(sp=z_at(k)), device_id_type=MESH)
+    for f in (left, right):
+        pl.semaphore_signal(barrier, inc=1, device_id=peer(fs=f), device_id_type=MESH)
+    pl.semaphore_signal(barrier, inc=1, device_id=sibling, device_id_type=MESH)
+    pl.semaphore_wait(barrier, n_sp + 2)
 
     sent = []
 
-    def remote(src, dst, recv, to, start=True):
-        copy = pltpu.make_async_remote_copy(
-            src_ref=src, dst_ref=dst, send_sem=send_sem.at[len(sent) if start else 0], recv_sem=recv, device_id=to,
-            device_id_type=MESH,
+    def remote(src, dst, send, recv, to):
+        return pltpu.make_async_remote_copy(
+            src_ref=src, dst_ref=dst, send_sem=send, recv_sem=recv, device_id=to, device_id_type=MESH,
         )
-        if start:
+
+    def push(src, dst, recv, to):
+        copy = remote(src, dst, send_sem.at[len(sent)], recv, to)
+        copy.start()
+        sent.append(copy)
+
+    def arrived(ref, recv):
+        remote(ref, ref, send_sem.at[0], recv, sibling).wait_recv()
+
+    def tok_piece(ref, c):
+        return ref.at[pl.ds(c * sub, sub)]
+
+    def token_slot(s, t, c):
+        return tok_piece(tokens.at[s * 2 + t], c)
+
+    def own_tokens(send, to):
+        return [
+            remote(tok_piece(tok, c), token_slot(sp, tp, c), send.at[c], tok_z.at[sp, c], to)
+            for c in range(TOKEN_PIECES)
+        ]
+
+    def own_up():
+        return own_tokens(own_send.at[0], peer(sp=sp + 1))
+
+    def own_down():
+        return own_tokens(own_send.at[1], peer(sp=sp - 1))
+
+    def to_sibling(s, c, src=None):
+        slot = token_slot(s, tp, c)
+        return remote(slot if src is None else src, slot, tok_t_send.at[s, c], tok_t.at[s, c], sibling)
+
+    def relayed(s, c, send, to):
+        slot = token_slot(s, tp, c)
+        return remote(slot, slot, send.at[s, c], tok_z.at[s, c], to)
+
+    def start_all(copies):
+        for copy in copies:
             copy.start()
-            sent.append(copy)
-        return copy
-
-    near = sorted(range(1, n_sp), key=lambda d: min(d, n_sp - d))
-    for d in near:
-        to = peer(sp=z_at(d))
-        ins, outs = weight_sources(z_at(d))
-        for i, (ref, at, width) in enumerate(ins):
-            remote(ref, in_piece(sp, fs, at, width), win_z.at[d, i], to)
-        for i, (ref, at, width) in enumerate(outs):
-            remote(ref, out_piece(sp, fs, at, width), wout_z.at[d, i], to)
-        remote(tok, tokens.at[sp * 2 + tp], tok_z.at[d], to)
-        remote(rate.at[z_at(d)], rates.at[sp], rate_z.at[d], to)
-    remote(tok, tokens.at[sp * 2 + tp], tok_t.at[0], peer(tp=other))
+
+    for k in range(1, n_sp):
+        push(rate, rates.at[sp], rate_z.at[k], peer(sp=z_at(k)))
+    for k in range(1, n_sp):
+        to = peer(sp=z_at(k))
+        for i, (ref, at, width) in enumerate(in_sources(z_at(k))):
+            push(ref, in_piece(sp, fs, at, width), win_z.at[k, i], to)
+    for c in range(TOKEN_PIECES):
+        to_sibling(sp, c, tok_piece(tok, c)).start()
+
+    @pl.when(sp == 0)
+    def _():
+        start_all(own_up())
+
+    @pl.when(sp > 0)
+    def _():
+        start_all(own_down())
+
+    for k in range(1, n_sp):
+        to = peer(sp=z_at(k))
+        for i, (ref, at, width) in enumerate(out_sources(z_at(k))):
+            push(ref, out_piece(sp, fs, at, width), wout_z.at[k, i], to)
 
     for copy in local:
         copy.wait()
 
-    def spread(d):
-        s = z_at(n_sp - d)
-        for e in range(1, n_fs):
-            remote(in_slot(s, fs), in_slot(s, fs), win_f.at[e, d], peer(fs=f_at(e)))
-        for e in range(1, n_fs):
-            remote(out_slot(s, fs), out_slot(s, fs), wout_f.at[e, d], peer(fs=f_at(e)))
-
-    spread(0)
-    for d in near:
-        s = z_at(n_sp - d)
-        me = peer(tp=other)
+    def z_in(k):
         for i, (ref, at, width) in enumerate(parts):
-            piece = in_piece(s, fs, at, width)
-            remote(piece, piece, win_z.at[d, i], me, start=False).wait_recv()
+            arrived(in_piece(z_at(k), fs, at, width), win_z.at[k, i])
+
+    def z_out(k):
         for i, (at, width) in enumerate(((0, rec), (rec, con))):
-            piece = out_piece(s, fs, at, width)
-            remote(piece, piece, wout_z.at[d, i], me, start=False).wait_recv()
-        spread(d)
-        piece = tokens.at[s * 2 + tp]
-        remote(piece, piece, tok_z.at[d], me, start=False).wait_recv()
-        remote(piece, piece, tok_t.at[d], me)
-        remote(rates.at[s], rates.at[s], rate_z.at[d], me, start=False).wait_recv()
-    for d in range(n_sp):
-        s = z_at((n_sp - d) % n_sp)
-        piece = tokens.at[s * 2 + other]
-        remote(piece, piece, tok_t.at[d], peer(tp=other), start=False).wait_recv()
-    for d in range(n_sp):
-        s = z_at((n_sp - d) % n_sp)
-        for e in range(1, n_fs):
-            f = f_at(n_fs - e)
-            remote(in_slot(s, f), in_slot(s, f), win_f.at[e, d], peer(tp=other), start=False).wait_recv()
-            remote(out_slot(s, f), out_slot(s, f), wout_f.at[e, d], peer(tp=other), start=False).wait_recv()
-    for copy in sent:
-        copy.wait_send()
+            arrived(out_piece(z_at(k), fs, at, width), wout_z.at[k, i])
+
+    def ring_in(k):
+        piece = in_rows(z_at(k), fs, 0, rows)
+        push(piece, piece, win_f.at[0, k], peer(fs=right))
+        push(piece, piece, win_f.at[1, k], peer(fs=left))
+
+    def ring_in_on(k):
+        s, half = z_at(k), rows // 2
+        arrived(in_rows(s, left, 0, rows), win_f.at[0, k])
+        piece = in_rows(s, left, 0, half)
+        push(piece, piece, win_f.at[2, k], peer(fs=right))
+        arrived(in_rows(s, right, 0, rows), win_f.at[1, k])
+        piece = in_rows(s, right, half, half)
+        push(piece, piece, win_f.at[3, k], peer(fs=left))
+
+    def ring_in_end(k):
+        s, half = z_at(k), rows // 2
+        arrived(in_rows(s, across, 0, half), win_f.at[2, k])
+        arrived(in_rows(s, across, half, half), win_f.at[3, k])
+
+    depth = rec + con
+
+    def ring_out(k):
+        piece = out_piece(z_at(k), fs, 0, depth)
+        push(piece, piece, wout_f.at[0, k], peer(fs=right))
+        push(piece, piece, wout_f.at[1, k], peer(fs=left))
+
+    def ring_out_copies(k):
+        s, half = z_at(k), depth // 2
+        near = out_piece(s, left, 0, half)
+        far = out_piece(s, right, half, half)
+        return (
+            remote(near, near, up_send.at[0, n_sp + k], wout_f.at[2, k], peer(fs=right)),
+            remote(far, far, up_send.at[1, n_sp + k], wout_f.at[3, k], peer(fs=left)),
+        )
+
+    def ring_out_on(k):
+        s = z_at(k)
+        first, second = ring_out_copies(k)
+        arrived(out_piece(s, left, 0, depth), wout_f.at[0, k])
+        first.start()
+        arrived(out_piece(s, right, 0, depth), wout_f.at[1, k])
+        second.start()
+
+    def ring_out_end(k):
+        s, half = z_at(k), depth // 2
+        arrived(out_piece(s, across, 0, half), wout_f.at[2, k])
+        arrived(out_piece(s, across, half, half), wout_f.at[3, k])
+
+    def relay_up(s):
+        for c in range(TOKEN_PIECES):
+            arrived(token_slot(s, tp, c), tok_z.at[s, c])
+
+            @pl.when(sp < n_sp - 1)
+            def _():
+                relayed(s, c, down_send, peer(sp=sp + 1)).start()
+
+            to_sibling(s, c).start()
+
+    def relay_down(s):
+        for c in range(TOKEN_PIECES):
+            arrived(token_slot(s, tp, c), tok_z.at[s, c])
+
+            @pl.when(sp > 0)
+            def _():
+                relayed(s, c, down_send, peer(sp=sp - 1)).start()
+
+            to_sibling(s, c).start()
+
+    def relays(j):
+        later_up = jnp.logical_and(j < sp, sp > 1)
+
+        @pl.when(later_up)
+        def _():
+            relay_up(j)
+
+        @pl.when(jnp.logical_and(later_up, jnp.logical_and(j == sp - 1, sp < n_sp - 1)))
+        def _():
+            start_all(own_up())
+
+        later = sp + 1 + j
+
+        @pl.when(later < n_sp)
+        def _():
+            relay_down(later)
+
+    ring_in(0)
+    for k in range(1, n_sp):
+        if k == n_sp - 1:
+            @pl.when(sp == 1)
+            def _():
+                relay_up(0)
+                start_all(own_up())
+
+        z_in(k)
+        ring_in(k)
+        ring_in_on(k - 1)
+    ring_in_on(n_sp - 1)
+    for k in range(n_sp):
+        if k:
+            z_out(k)
+        ring_out(k)
+    for k in range(1, n_sp):
+        arrived(rates.at[z_at(k)], rate_z.at[k])
+    for k in range(n_sp):
+        ring_in_end(k)
 
     for h in range(heads):
-        state[h] = init[sp * heads + h].T
+        state[h] = first_state[h].T
     ext[0:8] = jnp.zeros((8, con), F32)
     lane_rec = pl.ds(pl.multiple_of(sp * rec, rec), rec)
     lane_con = pl.ds(pl.multiple_of(sp * con, con), con)
@@ -346,33 +479,73 @@
     upper = (row_id <= col_id).astype(F32)
     length = 2 * span
 
-    def sib_copy(s):
-        return pltpu.make_async_remote_copy(
-            src_ref=sib_send.at[s], dst_ref=sib_recv.at[s], send_sem=rs_send.at[0, s],
-            recv_sem=sib_sem.at[s], device_id=peer(tp=other), device_id_type=MESH,
+    def sib_copy(s, c):
+        return remote(sib_send.at[s, c], sib_recv.at[s, c], sib_out.at[s, c], sib_sem.at[s, c], sibling)
+
+    def z_copy(s, c):
+        return remote(z_send.at[s, c], z_recv.at[sp, c], rs_send.at[s, c], zr_sem.at[sp, c], peer(sp=s))
+
+    def edge_copy(s, c, to):
+        return remote(z_send.at[s, c], rl_recv.at[s, c], rs_send.at[s, c], rl_sem.at[s, c], peer(sp=to))
+
+    def through_low(s):
+        return jnp.logical_and(sp == 0, s >= 2)
+
+    def through_high(s):
+        return jnp.logical_and(sp == n_sp - 1, s <= n_sp - 3)
+
+    def joins(s):
+        return jnp.logical_or(
+            jnp.logical_and(sp == 1, s >= 2), jnp.logical_and(sp == n_sp - 2, s <= n_sp - 3)
         )
 
-    def z_copy(s):
-        d = lax.rem(s - sp + n_sp, n_sp)
-        return pltpu.make_async_remote_copy(
-            src_ref=z_send.at[s], dst_ref=z_recv.at[d], send_sem=rs_send.at[1, d],
-            recv_sem=zr_sem.at[d], device_id=peer(sp=s), device_id_type=MESH,
-        )
+    def plain(s):
+        edge = jnp.logical_or(through_low(s), through_high(s))
+        return jnp.logical_not(jnp.logical_or(jnp.logical_or(edge, joins(s)), s == sp))
 
     def pass_on(s):
-        sib_copy(s).wait_recv()
-        total = mine[s] + sib_recv[s].astype(F32)
-
-        @pl.when(s != sp)
-        def _():
-            z_send[s] = total.astype(BF16)
-            z_copy(s).start()
-
-        @pl.when(s == sp)
-        def _():
-            z_recv[0] = total.astype(BF16)
+        for c in range(chunks):
+            sib_copy(s, c).wait_recv()
+            total = mine[s, c] + sib_recv[s, c].astype(F32)
+            mine[s, c] = total
+
+            @pl.when(jnp.logical_not(jnp.logical_or(joins(s), s == sp)))
+            def _():
+                z_send[s, c] = total.astype(BF16)
+
+            @pl.when(plain(s))
+            def _():
+                z_copy(s, c).start()
+
+            @pl.when(through_low(s))
+            def _():
+                edge_copy(s, c, 1).start()
+
+            @pl.when(through_high(s))
+            def _():
+                edge_copy(s, c, n_sp - 2).start()
+
+    def join(s):
+        for c in range(chunks):
+            arrived(rl_recv.at[s, c], rl_sem.at[s, c])
+            z_send[s, c] = (mine[s, c] + rl_recv[s, c].astype(F32)).astype(BF16)
+            z_copy(s, c).start()
+
+    def project_out(s):
+        for c in range(chunks):
+            partial = jnp.dot(
+                both[s], wout[:, c * chunk : (c + 1) * chunk], preferred_element_type=F32
+            )
+            first = partial[:span]
+            second = partial[span:]
+            mine[s, c] = jnp.where(tp == 0, first, second)
+            sib_send[s, c] = jnp.where(tp == 0, second, first).astype(BF16)
+            sib_copy(s, c).start()
 
     def step(s, carry):
+        relays(s)
+        for c in range(TOKEN_PIECES):
+            arrived(token_slot(s, other, c), tok_t.at[s, c])
         block = jnp.concatenate([tokens[2 * s], tokens[2 * s + 1]], axis=0)
 
         def project(at, width):
@@ -389,11 +562,15 @@
         key_gate = headroom[:, lane_rec] * jax.nn.sigmoid(-forget)
         log_forget = jnp.log1p(-key_gate)
         gains = gain[:, lane_rec]
+        mine_rate = [rates[s, pl.ds(sp * heads + h, 1), :] for h in range(heads)]
+        if heads < 8:
+            mine_rate.append(jnp.zeros((8 - heads, 2 * span), F32))
+        mine_rate = jnp.concatenate(mine_rate, axis=0)
         halves = []
         for c in range(2):
             part = slice(c * span, (c + 1) * span)
             cum = jnp.dot(lower, log_forget[part], precision=lax.Precision.HIGHEST)
-            extra = jnp.dot(rates[s][:, part], upper, precision=lax.Precision.HIGHEST)
+            extra = jnp.dot(mine_rate[:, part], upper, precision=lax.Precision.HIGHEST)
             extra_t = extra.T
             grow = jnp.exp(cum)
             query_grow = query[part] * grow
@@ -433,40 +610,90 @@
             conv = conv + taps[j : j + 1, lane_con] * ext[pl.ds(8 - (KW - 1) + j, length)]
         ext[0:8] = ext[length:]
         conv_out = (conv_gate * conv).astype(BF16)
-        both = jnp.concatenate([jnp.concatenate(halves, axis=0), conv_out], axis=1)
-        chunk = min(512, wide)
-        for n in range(0, wide, chunk):
-            partial = jnp.dot(both, wout[:, n : n + chunk], preferred_element_type=F32)
-            first = partial[:span]
-            second = partial[span:]
-            mine[s, :, n : n + chunk] = jnp.where(tp == 0, first, second)
-            sib_send[s, :, n : n + chunk] = jnp.where(tp == 0, second, first).astype(BF16)
-        sib_copy(s).start()
+        both[s] = jnp.concatenate([jnp.concatenate(halves, axis=0), conv_out], axis=1)
+
+        @pl.when(s == 0)
+        def _():
+            for k in range(n_sp):
+                ring_out_on(k)
+
+        @pl.when(s == 1)
+        def _():
+            for k in range(n_sp):
+                ring_out_end(k)
 
         @pl.when(s > 0)
         def _():
+            project_out(s - 1)
             pass_on(s - 1)
 
         return carry
 
     lax.fori_loop(0, n_sp, step, 0)
+    project_out(n_sp - 1)
     pass_on(n_sp - 1)
-    for d in range(1, n_sp):
-        pltpu.make_async_remote_copy(
-            src_ref=z_recv.at[d], dst_ref=z_recv.at[d], send_sem=rs_send.at[1, d],
-            recv_sem=zr_sem.at[d], device_id=peer(tp=other), device_id_type=MESH,
-        ).wait_recv()
-    total = z_recv[0].astype(F32)
-    for d in range(1, n_sp):
-        total = total + z_recv[d].astype(F32)
-    out[...] = total.astype(BF16)
+
+    @pl.when(sp == 1)
+    def _():
+        for s in range(2, n_sp):
+            join(s)
+
+    @pl.when(sp == n_sp - 2)
+    def _():
+        for s in range(n_sp - 2):
+            join(s)
+
+    for d in range(n_sp):
+        comes = sp != d
+        if d == 0:
+            comes = jnp.logical_and(comes, sp < 2)
+        if d == n_sp - 1:
+            comes = jnp.logical_and(comes, sp > n_sp - 3)
+
+        @pl.when(comes)
+        def _():
+            for c in range(chunks):
+                arrived(z_recv.at[d, c], zr_sem.at[d, c])
+                mine[sp, c] = mine[sp, c] + z_recv[d, c].astype(F32)
+
+    for c in range(chunks):
+        out[:, c * chunk : (c + 1) * chunk] = mine[sp, c].astype(BF16)
+
+    for copy in sent:
+        copy.wait_send()
+    for k in range(n_sp):
+        for copy in ring_out_copies(k):
+            copy.wait_send()
+
+    @pl.when(sp < n_sp - 1)
+    def _():
+        for copy in own_up():
+            copy.wait_send()
+
+    @pl.when(sp > 0)
+    def _():
+        for copy in own_down():
+            copy.wait_send()
+
     for s in range(n_sp):
-        sib_copy(s).wait_send()
-    for d in range(1, n_sp):
-        pltpu.make_async_remote_copy(
-            src_ref=z_send.at[z_at(d)], dst_ref=z_recv.at[d], send_sem=rs_send.at[1, d],
-            recv_sem=zr_sem.at[d], device_id=peer(sp=z_at(d)), device_id_type=MESH,
-        ).wait_send()
+        for c in range(TOKEN_PIECES):
+            to_sibling(s, c).wait_send()
+            forwarded = jnp.logical_or(
+                jnp.logical_and(sp > s, sp < n_sp - 1), jnp.logical_and(sp < s, sp > 0)
+            )
+
+            @pl.when(forwarded)
+            def _():
+                relayed(s, c, down_send, sibling).wait_send()
+
+        for c in range(chunks):
+            sib_copy(s, c).wait_send()
+
+            @pl.when(sp != s)
+            def _():
+                remote(
+                    z_send.at[s, c], rl_recv.at[s, c], rs_send.at[s, c], rl_sem.at[s, c], sibling
+                ).wait_send()
 
 
 def sequence_shards(n_sp, n_fs, *arrays):
@@ -474,46 +701,55 @@
     span, wide = tok.shape[1:]
     rec, con = wq.shape[1] // n_sp, cg.shape[1] // n_sp
     heads = rec // DK
-    by_place = rate[0].reshape(n_sp, heads, rate.shape[2])
-    by_place = jnp.pad(by_place, ((0, 0), (0, 8 - heads), (0, 0)))
+    chunk = wide // OUT_PIECES
     hbm = pl.BlockSpec(memory_space=pl.ANY)
     vmem = pl.BlockSpec(memory_space=pltpu.VMEM)
     dma = pltpu.SemaphoreType.DMA
+    flat = (n_sp, OUT_PIECES, span, chunk)
     mixed = pl.pallas_call(
         functools.partial(layer_kernel, n_sp, n_fs),
         out_shape=jax.ShapeDtypeStruct((span, wide), BF16),
-        in_specs=[hbm] * 9 + [vmem, hbm] + [vmem] * 4,
+        in_specs=[hbm] * 11 + [vmem] * 4,
         out_specs=vmem,
         scratch_shapes=[
             pltpu.VMEM((2 * n_sp, span, wide), BF16),
             pltpu.VMEM((wide, 3 * (rec + con)), BF16),
             pltpu.VMEM((rec + con, wide), BF16),
-            pltpu.VMEM((n_sp, 8, rate.shape[2]), F32),
+            pltpu.VMEM((n_sp,) + rate.shape[1:], F32),
+            pltpu.VMEM((heads, DK, DK), F32),
             pltpu.VMEM((heads, DK, DK), F32),
             pltpu.VMEM((8 + 2 * span, con), F32),
-            pltpu.VMEM((n_sp, span, wide), BF16),
-            pltpu.VMEM((n_sp, span, wide), BF16),
-            pltpu.VMEM((n_sp, span, wide), F32),
-            pltpu.VMEM((n_sp, span, wide), BF16),
-            pltpu.VMEM((n_sp, span, wide), BF16),
-            dma((10,)),
-            dma(((n_sp - 1) * 10 + n_sp * (1 + 2 * (n_fs - 1)),)),
+            pltpu.VMEM((n_sp, 2 * span, rec + con), BF16),
+            pltpu.VMEM(flat, BF16),
+            pltpu.VMEM(flat, BF16),
+            pltpu.VMEM(flat, F32),
+            pltpu.VMEM(flat, BF16),
+            pltpu.VMEM(flat, BF16),
+            pltpu.VMEM(flat, BF16),
+            dma((11,)),
+            dma(((n_sp - 1) * 9 + n_sp * 6,)),
             dma((n_sp, 6)),
             dma((n_sp, 2)),
-            dma((n_fs, n_sp)),
-            dma((n_fs, n_sp)),
+            dma((4, n_sp)),
+            dma((4, n_sp)),
+            dma((n_sp, TOKEN_PIECES)),
+            dma((n_sp, TOKEN_PIECES)),
             dma((n_sp,)),
-            dma((n_sp,)),
-            dma((n_sp,)),
-            dma((n_sp,)),
-            dma((n_sp,)),
-            dma((2, n_sp)),
+            dma((2, 2 * n_sp)),
+            dma((n_sp, TOKEN_PIECES)),
+            dma((2, TOKEN_PIECES)),
+            dma((n_sp, TOKEN_PIECES)),
+            dma((n_sp, OUT_PIECES)),
+            dma((n_sp, OUT_PIECES)),
+            dma((n_sp, OUT_PIECES)),
+            dma((n_sp, OUT_PIECES)),
+            dma((n_sp, OUT_PIECES)),
         ],
         compiler_params=pltpu.CompilerParams(
             collective_id=0, has_side_effects=True, vmem_limit_bytes=60 * 2**20
         ),
     )(
-        tok[0], wq, wf, wv, cg, cm, ci, ro, co, headroom[None], by_place, init[0], gain[None],
+        tok[0], wq, wf, wv, cg, cm, ci, ro, co, rate[0], init[0], headroom[None], gain[None],
         taps, bias[None],
     )
     return mixed[None]
@@ -526,9 +762,14 @@
     span = arrays[0].shape[1]
     even = (
         sizes["tp"] == 2
+        and n_fs == 4
+        and n_sp >= 4
+        and n_sp & (n_sp - 1) == 0
+        and arrays[0].shape[2] % (128 * OUT_PIECES) == 0
         and arrays[0].shape[0] == 1
         and rec % (n_sp * DK) == 0
         and rec // (n_sp * DK) <= 8
+        and arrays[8].shape[1] % 8 == 0
         and con % (n_sp * 128) == 0
         and rows % 128 == 0
         and span == DK

time: 150 us -> 128 us (0.85)
  Pallas kernels: 147 us -> 126 us
    pallas_call x1, Pallas kernels: 147 us -> 126 us  [sequence_shards(): pl.pallas_call(functools.partial(layer_kernel, n_sp, n_fs), out_shape=jax...]
where the time goes in v1:
time: 128 us
  Pallas kernels  126 us (98%)
  local copies, waits for them, and re-layouts  1.88 us (1%)
    pallas_call x1, Pallas kernels, sequence_shards(): pl.pallas_call(functools.partial(layer_kernel, n_sp, n_fs), out_shape=jax...  126 us

profile of v1, /device:TPU:28, one launch (start us, length us, event | category | flops | bytes accessed | tf_op | source)
XLA Modules:
  0.0 128.0 jit_solution(209196409879575628)
XLA Ops:
  0.0 126.1 %shard_map.145 = bf16[128,2048]{1,0:T(8,128)(2,1)} custom-call(bf16[128,2048]{1,0:T(8,128)(2,1)} %bitcast.8, bf16[128,1024]{1,0:T(8,128)(2,1)} %wq.1, bf16[128,1024]{1,0:T(8,128)(2,1)} %wf.1, bf16[128,1024]{1,0:T(8,128)(2,1)} %wv.1, bf16[128,512]{1,0:T(8,128)(2,1)} %cg.1, bf16[128,512]{1,0:T(8,128)(2,1)} %cm.1, bf16[128,512]{1,0:T(8,128)(2,1)} %ci.1, ...), custom_call_target="tpu_custom_call" | custom-call | tf_op jit(solution)/shard_map/pallas_call | solution.py:709
  126.1 1.9 %copy.17 = bf16[1,128,2048]{2,1,0:T(8,128)(2,1)} copy(bf16[1,128,2048]{2,1,0:T(8,128)(2,1)} %bitcast.7) | data formatting | bytes 1048576

commit v2 on v1

--- a/solution.py
+++ b/solution.py
@@ -199,8 +199,9 @@
 
 def layer_kernel(
     n_sp, n_fs, tok, wq, wf, wv, cg, cm, ci, ro, co, rate, init, headroom, gain, taps, bias,
-    out, tokens, win, wout, rates, first_state, state, ext, both, sib_send, sib_recv, mine, z_send,
-    z_recv, rl_recv, loc_sem, send_sem, win_z, wout_z, win_f, wout_f, tok_z, tok_t, rate_z, up_send,
+    out, tokens, win, wcon, wout, rates, first_state, state, ext, both, sib_send, sib_recv, mine,
+    z_send, z_recv, rl_recv, stage_in, stage_con, stage_out, loc_in, loc_con, loc_out, loc_sem,
+    send_sem, in_send, win_z, wcon_z, wout_z, win_f, late_f, tok_z, tok_t, rate_z, ring_send, late_send,
     down_send, own_send, tok_t_send, sib_sem, sib_out, zr_sem, rl_sem, rs_send,
 ):
     sp, fs, tp = lax.axis_index("sp"), lax.axis_index("fs"), lax.axis_index("tp")
@@ -214,17 +215,10 @@
     lanes_out = ro.shape[1]
     chunks, chunk = mine.shape[1], mine.shape[3]
     sub = span // TOKEN_PIECES
+    shards_in = chunk // lanes_out
 
     def peer(**where):
         return {"sp": where.get("sp", sp), "fs": where.get("fs", fs), "tp": where.get("tp", tp)}
-
-    def z_at(k):
-        place, bit = sp, 1
-        while bit < n_sp:
-            if k & bit:
-                place = place + bit * (1 - 2 * lax.rem(sp // bit, 2))
-            bit *= 2
-        return place
 
     half_ring = n_fs // 2
 
@@ -237,47 +231,59 @@
     across = ring(lax.rem(at_ring + 2, n_fs))
     sibling = peer(tp=other)
 
-    parts = []
-    at = 0
-    for ref, width in ((wq, rec), (wf, rec), (wv, rec), (cg, con), (cm, con), (ci, con)):
-        parts.append((ref, at, width))
-        at += width
+    rec_parts = [(ref, i * rec, rec) for i, ref in enumerate((wq, wf, wv))]
+    con_parts = [(ref, i * con, con) for i, ref in enumerate((cg, cm, ci))]
 
     def in_rows(s, f, first, count):
         return win.at[pl.ds(pl.multiple_of((s * n_fs + f) * rows + first, count), count)]
 
-    def in_piece(s, f, at, width):
-        first = pl.multiple_of((s * n_fs + f) * rows, rows)
-        return win.at[pl.ds(first, rows), pl.ds(at, width)]
-
-    def out_piece(s, f, at, width):
-        first = pl.multiple_of((s * n_fs + f) * lanes_out, lanes_out)
-        return wout.at[pl.ds(at, width), pl.ds(first, lanes_out)]
-
-    def in_sources(s):
-        return [
-            (ref.at[:, pl.ds(pl.multiple_of(s * width, width), width)], at, width)
-            for ref, at, width in parts
-        ]
-
-    def out_sources(s):
-        return [
-            (ro.at[pl.ds(pl.multiple_of(s * rec, rec), rec)], 0, rec),
-            (co.at[pl.ds(pl.multiple_of(s * con, con), con)], rec, con),
-        ]
-
-    local = [(ref, in_piece(sp, fs, at, width)) for ref, at, width in in_sources(sp)]
-    local += [(ref, out_piece(sp, fs, at, width)) for ref, at, width in out_sources(sp)]
-    local.append((tok, tokens.at[sp * 2 + tp]))
-    local.append((rate, rates.at[sp]))
-    local.append((init.at[pl.ds(sp * heads, heads)], first_state))
-    local = [pltpu.make_async_copy(*pair, loc_sem.at[i]) for i, pair in enumerate(local)]
-    for copy in local:
+    def con_rows(s, f):
+        return wcon.at[pl.ds(pl.multiple_of((s * n_fs + f) * rows, rows), rows)]
+
+    def out_slot(s, f):
+        return wout.at[s * n_fs + f]
+
+    def stage(z, in_to, con_to, out_to, place):
+        copies = []
+        for some, to, sem in ((rec_parts, in_to, loc_in), (con_parts, con_to, loc_con)):
+            for ref, at, width in some:
+                src = ref.at[:, pl.ds(pl.multiple_of(z * width, width), width)]
+                copies.append((src, to.at[:, pl.ds(at, width)], sem.at[place]))
+        for ref, at, width in ((ro, 0, rec), (co, rec, con)):
+            src = ref.at[pl.ds(pl.multiple_of(z * width, width), width)]
+            copies.append((src, out_to.at[pl.ds(at, width)], loc_out.at[place]))
+        return [pltpu.make_async_copy(*copy) for copy in copies]
+
+    below, above = sp, n_sp - 1 - sp
+    fewer = jnp.minimum(below, above)
+    upward = jnp.where(below < above, 1, -1)
+    edge = fewer == 0
+
+    def near(j):
+        paired = j <= 2 * fewer
+        side = jnp.where(paired, upward * (1 - 2 * (j % 2)), upward)
+        return sp + side * jnp.where(paired, (j + 1) // 2, j - fewer)
+
+    def to_send(j):
+        if j == 1:
+            return near(1)
+        return jnp.where(edge, near(n_sp + 1 - j), near(j))
+
+    local = []
+    for j in range(1, n_sp):
+        local += stage(to_send(j), stage_in.at[j], stage_con.at[j], stage_out.at[j], j)
+    local += stage(sp, in_rows(sp, fs, 0, rows), con_rows(sp, fs), out_slot(sp, fs), 0)
+    others = [
+        (tok, tokens.at[sp * 2 + tp]), (rate, rates.at[sp]),
+        (init.at[pl.ds(sp * heads, heads)], first_state),
+    ]
+    others = [pltpu.make_async_copy(*pair, loc_sem.at[i]) for i, pair in enumerate(others)]
+    for copy in local + others:
         copy.start()
 
     barrier = pltpu.get_barrier_semaphore()
-    for k in range(1, n_sp):
-        pl.semaphore_signal(barrier, inc=1, device_id=peer(sp=z_at(k)), device_id_type=MESH)
+    for j in range(1, n_sp):
+        pl.semaphore_signal(barrier, inc=1, device_id=peer(sp=near(j)), device_id_type=MESH)
     for f in (left, right):
         pl.semaphore_signal(barrier, inc=1, device_id=peer(fs=f), device_id_type=MESH)
     pl.semaphore_signal(barrier, inc=1, device_id=sibling, device_id_type=MESH)
@@ -328,142 +334,193 @@
         for copy in copies:
             copy.start()
 
-    for k in range(1, n_sp):
-        push(rate, rates.at[sp], rate_z.at[k], peer(sp=z_at(k)))
-    for k in range(1, n_sp):
-        to = peer(sp=z_at(k))
-        for i, (ref, at, width) in enumerate(in_sources(z_at(k))):
-            push(ref, in_piece(sp, fs, at, width), win_z.at[k, i], to)
+    def send_in(j):
+        z = to_send(j)
+        push(rate, rates.at[sp], rate_z.at[sp], peer(sp=z))
+        arrived(stage_in.at[j], loc_in.at[j])
+        push(stage_in.at[j], in_rows(sp, fs, 0, rows), win_z.at[sp], peer(sp=z))
+
+    def late_copies():
+        copies = []
+        for j in range(1, n_sp):
+            to = peer(sp=to_send(j))
+            copies.append(
+                remote(stage_con.at[j], con_rows(sp, fs), late_send.at[0, j], wcon_z.at[sp], to)
+            )
+            copies.append(
+                remote(stage_out.at[j], out_slot(sp, fs), late_send.at[1, j], wout_z.at[sp], to)
+            )
+        return copies
+
+    low, high = sp == 1, sp == n_sp - 2
+    send_in(1)
+
+    for j in range(2, n_sp):
+        send_in(j)
+    for j in range(n_sp):
+        arrived(stage_con.at[j] if j else con_rows(sp, fs), loc_con.at[j])
+        arrived(stage_out.at[j] if j else out_slot(sp, fs), loc_out.at[j])
+    start_all(late_copies()[:2])
+    for copy in others:
+        copy.wait()
+
+    @pl.when(sp == 0)
+    def _():
+        start_all(own_up())
+
+    @pl.when(sp == n_sp - 1)
+    def _():
+        start_all(own_down())
+
     for c in range(TOKEN_PIECES):
         to_sibling(sp, c, tok_piece(tok, c)).start()
 
-    @pl.when(sp == 0)
-    def _():
-        start_all(own_up())
-
-    @pl.when(sp > 0)
-    def _():
-        start_all(own_down())
-
-    for k in range(1, n_sp):
-        to = peer(sp=z_at(k))
-        for i, (ref, at, width) in enumerate(out_sources(z_at(k))):
-            push(ref, out_piece(sp, fs, at, width), wout_z.at[k, i], to)
-
-    for copy in local:
-        copy.wait()
-
-    def z_in(k):
-        for i, (ref, at, width) in enumerate(parts):
-            arrived(in_piece(z_at(k), fs, at, width), win_z.at[k, i])
-
-    def z_out(k):
-        for i, (at, width) in enumerate(((0, rec), (rec, con))):
-            arrived(out_piece(z_at(k), fs, at, width), wout_z.at[k, i])
+    arrived(in_rows(sp, fs, 0, rows), loc_in.at[0])
+
+    def z_in(j):
+        z = near(j)
+        arrived(in_rows(z, fs, 0, rows), win_z.at[z])
+        arrived(rates.at[z], rate_z.at[z])
+
+    def z_late(j):
+        z = near(j)
+        arrived(con_rows(z, fs), wcon_z.at[z])
+        arrived(out_slot(z, fs), wout_z.at[z])
+
+    def place(j):
+        return near(j) if j else sp
+
+    def in_ring(k):
+        s, half = place(k), rows // 2
+        whole = in_rows(s, fs, 0, rows)
+        copies = (
+            (whole, right), (whole, left), (in_rows(s, left, 0, half), right),
+            (in_rows(s, right, half, half), left),
+        )
+        return [
+            remote(piece, piece, in_send.at[i, k], win_f.at[i, k], peer(fs=to))
+            for i, (piece, to) in enumerate(copies)
+        ]
 
     def ring_in(k):
-        piece = in_rows(z_at(k), fs, 0, rows)
-        push(piece, piece, win_f.at[0, k], peer(fs=right))
-        push(piece, piece, win_f.at[1, k], peer(fs=left))
+        start_all(in_ring(k)[:2])
 
     def ring_in_on(k):
-        s, half = z_at(k), rows // 2
+        s = place(k)
+        on = in_ring(k)[2:]
         arrived(in_rows(s, left, 0, rows), win_f.at[0, k])
-        piece = in_rows(s, left, 0, half)
-        push(piece, piece, win_f.at[2, k], peer(fs=right))
+        on[0].start()
         arrived(in_rows(s, right, 0, rows), win_f.at[1, k])
-        piece = in_rows(s, right, half, half)
-        push(piece, piece, win_f.at[3, k], peer(fs=left))
+        on[1].start()
 
     def ring_in_end(k):
-        s, half = z_at(k), rows // 2
+        s, half = place(k), rows // 2
         arrived(in_rows(s, across, 0, half), win_f.at[2, k])
         arrived(in_rows(s, across, half, half), win_f.at[3, k])
 
-    depth = rec + con
-
-    def ring_out(k):
-        piece = out_piece(z_at(k), fs, 0, depth)
-        push(piece, piece, wout_f.at[0, k], peer(fs=right))
-        push(piece, piece, wout_f.at[1, k], peer(fs=left))
-
-    def ring_out_copies(k):
-        s, half = z_at(k), depth // 2
-        near = out_piece(s, left, 0, half)
-        far = out_piece(s, right, half, half)
-        return (
-            remote(near, near, up_send.at[0, n_sp + k], wout_f.at[2, k], peer(fs=right)),
-            remote(far, far, up_send.at[1, n_sp + k], wout_f.at[3, k], peer(fs=left)),
+    def late_ring(k):
+        s = place(k)
+        mine_con, mine_out = con_rows(s, fs), out_slot(s, fs)
+        passed_con, passed_out = con_rows(s, left), out_slot(s, right)
+        copies = (
+            (mine_con, right), (mine_out, left), (mine_con, left), (mine_out, right),
+            (passed_con, right), (passed_out, left),
         )
-
-    def ring_out_on(k):
-        s = z_at(k)
-        first, second = ring_out_copies(k)
-        arrived(out_piece(s, left, 0, depth), wout_f.at[0, k])
-        first.start()
-        arrived(out_piece(s, right, 0, depth), wout_f.at[1, k])
-        second.start()
-
-    def ring_out_end(k):
-        s, half = z_at(k), depth // 2
-        arrived(out_piece(s, across, 0, half), wout_f.at[2, k])
-        arrived(out_piece(s, across, half, half), wout_f.at[3, k])
-
-    def relay_up(s):
-        for c in range(TOKEN_PIECES):
-            arrived(token_slot(s, tp, c), tok_z.at[s, c])
-
-            @pl.when(sp < n_sp - 1)
-            def _():
-                relayed(s, c, down_send, peer(sp=sp + 1)).start()
-
-            to_sibling(s, c).start()
-
-    def relay_down(s):
-        for c in range(TOKEN_PIECES):
-            arrived(token_slot(s, tp, c), tok_z.at[s, c])
-
-            @pl.when(sp > 0)
-            def _():
-                relayed(s, c, down_send, peer(sp=sp - 1)).start()
-
-            to_sibling(s, c).start()
-
-    def relays(j):
-        later_up = jnp.logical_and(j < sp, sp > 1)
-
-        @pl.when(later_up)
+        return [
+            remote(piece, piece, ring_send.at[i, k], late_f.at[i, k], peer(fs=to))
+            for i, (piece, to) in enumerate(copies)
+        ]
+
+    def ring_late(k):
+        start_all(late_ring(k)[:4])
+
+    def ring_late_on(k):
+        s = place(k)
+        on = late_ring(k)[4:]
+        arrived(con_rows(s, left), late_f.at[0, k])
+        on[0].start()
+        arrived(out_slot(s, right), late_f.at[1, k])
+        on[1].start()
+
+    def ring_late_end(k):
+        s = place(k)
+        arrived(con_rows(s, right), late_f.at[2, k])
+        arrived(out_slot(s, left), late_f.at[3, k])
+        arrived(con_rows(s, across), late_f.at[4, k])
+        arrived(out_slot(s, across), late_f.at[5, k])
+
+    def relay(s, c, step_by):
+        arrived(token_slot(s, tp, c), tok_z.at[s, c])
+        if step_by:
+            relayed(s, c, down_send, peer(sp=sp + step_by)).start()
+        to_sibling(s, c).start()
+
+    def relays(when, s, step_by, pieces=range(TOKEN_PIECES)):
+        @pl.when(when)
         def _():
-            relay_up(j)
-
-        @pl.when(jnp.logical_and(later_up, jnp.logical_and(j == sp - 1, sp < n_sp - 1)))
-        def _():
-            start_all(own_up())
-
-        later = sp + 1 + j
-
-        @pl.when(later < n_sp)
-        def _():
-            relay_down(later)
-
+            for c in pieces:
+                relay(s, c, step_by)
+
+    early, late = range(TOKEN_PIECES // 2), range(TOKEN_PIECES // 2, TOKEN_PIECES)
+    bottom, top = 0, n_sp - 1
+
+    def second_in():
+        z_in(2)
+        ring_in(2)
+
+    def first_late():
+        z_late(1)
+        ring_late(1)
+
+    inner = jnp.logical_not(edge)
     ring_in(0)
-    for k in range(1, n_sp):
-        if k == n_sp - 1:
-            @pl.when(sp == 1)
-            def _():
-                relay_up(0)
-                start_all(own_up())
-
-        z_in(k)
-        ring_in(k)
-        ring_in_on(k - 1)
-    ring_in_on(n_sp - 1)
-    for k in range(n_sp):
-        if k:
-            z_out(k)
-        ring_out(k)
-    for k in range(1, n_sp):
-        arrived(rates.at[z_at(k)], rate_z.at[k])
+    z_in(1)
+    ring_in(1)
+    pl.when(inner)(second_in)
+    ring_in_on(0)
+    ring_late(0)
+
+    @pl.when(low)
+    def _():
+        start_all(own_down())
+
+    @pl.when(high)
+    def _():
+        start_all(own_up())
+
+    ring_in_on(1)
+
+    @pl.when(edge)
+    def _():
+        first_late()
+        second_in()
+
+    z_in(3)
+    ring_in(3)
+    start_all(late_copies()[2:])
+
+    @pl.when(high)
+    def _():
+        start_all(own_down())
+
+    pl.when(inner)(first_late)
+    ring_in_on(2)
+    relays(low, bottom, 1, early)
+    relays(high, top, -1, early)
+    ring_in_on(3)
+    ring_late_on(0)
+    relays(low, bottom, 1, late)
+    relays(high, top, -1, late)
+
+    @pl.when(low)
+    def _():
+        start_all(own_up())
+
+    ring_late_on(1)
+    z_late(2)
+    ring_late(2)
+    z_late(3)
+    ring_late(3)
     for k in range(n_sp):
         ring_in_end(k)
 
@@ -533,8 +590,11 @@
 
     def project_out(s):
         for c in range(chunks):
+            columns = jnp.concatenate(
+                [wout[c * shards_in + i] for i in range(shards_in)], axis=1
+            )
             partial = jnp.dot(
-                both[s], wout[:, c * chunk : (c + 1) * chunk], preferred_element_type=F32
+                both[s], columns, preferred_element_type=F32
             )
             first = partial[:span]
             second = partial[span:]
@@ -542,8 +602,19 @@
             sib_send[s, c] = jnp.where(tp == 0, second, first).astype(BF16)
             sib_copy(s, c).start()
 
-    def step(s, carry):
-        relays(s)
+    def convolve(s):
+        block = jnp.concatenate([tokens[2 * s], tokens[2 * s + 1]], axis=0)
+        projected = jnp.dot(block, wcon[...], preferred_element_type=F32).astype(BF16).astype(F32)
+        prod = projected[:, con : 2 * con] * projected[:, 2 * con :]
+        ext[8:] = prod
+        conv = jnp.broadcast_to(bias[:, lane_con], prod.shape)
+        for j in range(KW):
+            conv = conv + taps[j : j + 1, lane_con] * ext[pl.ds(8 - (KW - 1) + j, length)]
+        ext[0:8] = ext[length:]
+        both[s, :, rec:] = (projected[:, :con] * conv).astype(BF16)
+
+    def recur(s):
+        relays(jnp.logical_and(edge, s != sp), s, 0)
         for c in range(TOKEN_PIECES):
             arrived(token_slot(s, other, c), tok_t.at[s, c])
         block = jnp.concatenate([tokens[2 * s], tokens[2 * s + 1]], axis=0)
@@ -556,9 +627,6 @@
         query = project(0, rec).astype(F32) * DK ** (-0.5)
         forget = project(rec, rec).astype(F32)
         value = project(2 * rec, rec)
-        base = 3 * rec
-        conv_gate = project(base, con).astype(F32)
-        prod = project(base + con, con).astype(F32) * project(base + 2 * con, con).astype(F32)
         key_gate = headroom[:, lane_rec] * jax.nn.sigmoid(-forget)
         log_forget = jnp.log1p(-key_gate)
         gains = gain[:, lane_rec]
@@ -604,34 +672,53 @@
                 square = jnp.mean(raw * raw, axis=-1, keepdims=True)
                 pieces.append((raw * lax.rsqrt(square + 1e-06) * gains[:, lanes]).astype(BF16))
             halves.append(jnp.concatenate(pieces, axis=1))
-        ext[8:] = prod
-        conv = jnp.broadcast_to(bias[:, lane_con], prod.shape)
-        for j in range(KW):
-            conv = conv + taps[j : j + 1, lane_con] * ext[pl.ds(8 - (KW - 1) + j, length)]
-        ext[0:8] = ext[length:]
-        conv_out = (conv_gate * conv).astype(BF16)
-        both[s] = jnp.concatenate([jnp.concatenate(halves, axis=0), conv_out], axis=1)
-
-        @pl.when(s == 0)
+        both[s, :, :rec] = jnp.concatenate(halves, axis=0)
+
+    lag = jnp.where(sp < 2, 0, 1)
+
+    def step(i, carry):
+        s = i - lag
+
+        @pl.when(jnp.logical_and(s >= 0, s < n_sp))
         def _():
+            recur(s)
+
+        @pl.when(i == 0)
+        def _():
+            ring_late_on(2)
+            relays(low, top - 1, -1)
+            relays(high, bottom, 1)
+            ring_late_on(3)
+
+        @pl.when(i == 1)
+        def _():
+            relays(low, top, -1)
+            relays(high, 1, 1)
             for k in range(n_sp):
-                ring_out_on(k)
-
-        @pl.when(s == 1)
+                ring_late_end(k)
+
+        @pl.when(jnp.logical_and(i == 1, lag == 0))
         def _():
-            for k in range(n_sp):
-                ring_out_end(k)
-
-        @pl.when(s > 0)
+            convolve(0)
+            project_out(0)
+            pass_on(0)
+
+        @pl.when(jnp.logical_and(i > 0, s < n_sp))
         def _():
-            project_out(s - 1)
-            pass_on(s - 1)
+            convolve(s)
+            project_out(s)
+
+        @pl.when(jnp.logical_and(jnp.logical_and(i > 0, s < n_sp), jnp.logical_or(s > 1, sp > 0)))
+        def _():
+            pass_on(s)
 
         return carry
 
-    lax.fori_loop(0, n_sp, step, 0)
-    project_out(n_sp - 1)
-    pass_on(n_sp - 1)
+    lax.fori_loop(0, n_sp + 1, step, 0)
+
+    @pl.when(sp == 0)
+    def _():
+        pass_on(1)
 
     @pl.when(sp == 1)
     def _():
@@ -659,10 +746,10 @@
     for c in range(chunks):
         out[:, c * chunk : (c + 1) * chunk] = mine[sp, c].astype(BF16)
 
-    for copy in sent:
+    for copy in sent + late_copies():
         copy.wait_send()
     for k in range(n_sp):
-        for copy in ring_out_copies(k):
+        for copy in in_ring(k) + late_ring(k):
             copy.wait_send()
 
     @pl.when(sp < n_sp - 1)
@@ -713,8 +800,9 @@
         out_specs=vmem,
         scratch_shapes=[
             pltpu.VMEM((2 * n_sp, span, wide), BF16),
-            pltpu.VMEM((wide, 3 * (rec + con)), BF16),
-            pltpu.VMEM((rec + con, wide), BF16),
+            pltpu.VMEM((wide, 3 * rec), BF16),
+            pltpu.VMEM((wide, 3 * con), BF16),
+            pltpu.VMEM((n_sp * n_fs, rec + con, wide // (n_sp * n_fs)), BF16),
             pltpu.VMEM((n_sp,) + rate.shape[1:], F32),
             pltpu.VMEM((heads, DK, DK), F32),
             pltpu.VMEM((heads, DK, DK), F32),
@@ -726,16 +814,25 @@
             pltpu.VMEM(flat, BF16),
             pltpu.VMEM(flat, BF16),
             pltpu.VMEM(flat, BF16),
-            dma((11,)),
-            dma(((n_sp - 1) * 9 + n_sp * 6,)),
-            dma((n_sp, 6)),
-            dma((n_sp, 2)),
+            pltpu.VMEM((n_sp, wide // (n_sp * n_fs), 3 * rec), BF16),
+            pltpu.VMEM((n_sp, wide // (n_sp * n_fs), 3 * con), BF16),
+            pltpu.VMEM((n_sp, rec + con, wide // (n_sp * n_fs)), BF16),
+            dma((n_sp,)),
+            dma((n_sp,)),
+            dma((n_sp,)),
+            dma((3,)),
+            dma(((n_sp - 1) * 2,)),
             dma((4, n_sp)),
+            dma((n_sp,)),
+            dma((n_sp,)),
+            dma((n_sp,)),
             dma((4, n_sp)),
+            dma((6, n_sp)),
             dma((n_sp, TOKEN_PIECES)),
             dma((n_sp, TOKEN_PIECES)),
             dma((n_sp,)),
-            dma((2, 2 * n_sp)),
+            dma((6, n_sp)),
+            dma((2, n_sp)),
             dma((n_sp, TOKEN_PIECES)),
             dma((2, TOKEN_PIECES)),
             dma((n_sp, TOKEN_PIECES)),
@@ -763,9 +860,8 @@
     even = (
         sizes["tp"] == 2
         and n_fs == 4
-        and n_sp >= 4
-        and n_sp & (n_sp - 1) == 0
-        and arrays[0].shape[2] % (128 * OUT_PIECES) == 0
+        and n_sp == 4
+        and arrays[0].shape[2] % (n_fs * n_sp * 128) == 0
         and arrays[0].shape[0] == 1
         and rec % (n_sp * DK) == 0
         and rec // (n_sp * DK) <= 8

time: 128 us -> 113 us (0.88)
  the two profiles are of different devices: /device:TPU:28 before, /device:TPU:0 now
where the time goes in v2:
time: 113 us
  Pallas kernels  111 us (98%)
  local copies, waits for them, and re-layouts  1.88 us (2%)
    pallas_call x1, Pallas kernels, sequence_shards(): pl.pallas_call(functools.partial(layer_kernel, n_sp, n_fs), out_shape=jax...  111 us

profile of v2, /device:TPU:0, one launch (start us, length us, event | category | flops | bytes accessed | tf_op | source)
XLA Modules:
  0.0 112.9 jit_solution(3772148840292312868)
XLA Ops:
  0.0 111.0 %shard_map.145 = bf16[128,2048]{1,0:T(8,128)(2,1)} custom-call(bf16[128,2048]{1,0:T(8,128)(2,1)} %bitcast.8, bf16[128,1024]{1,0:T(8,128)(2,1)} %wq.1, bf16[128,1024]{1,0:T(8,128)(2,1)} %wf.1, bf16[128,1024]{1,0:T(8,128)(2,1)} %wv.1, bf16[128,512]{1,0:T(8,128)(2,1)} %cg.1, bf16[128,512]{1,0:T(8,128)(2,1)} %cm.1, bf16[128,512]{1,0:T(8,128)(2,1)} %ci.1, ...), custom_call_target="tpu_custom_call" | custom-call | tf_op jit(solution)/shard_map/pallas_call | solution.py:796
  111.0 1.9 %copy.17 = bf16[1,128,2048]{2,1,0:T(8,128)(2,1)} copy(bf16[1,128,2048]{2,1,0:T(8,128)(2,1)} %bitcast.7) | data formatting | bytes 1048576

commit v3 on v2

--- a/solution.py
+++ b/solution.py
@@ -194,15 +194,18 @@
 CONTRACT_LAST = (((1,), (1,)), ((), ()))
 CONTRACT_FIRST = (((0,), (0,)), ((), ()))
 TOKEN_PIECES = 4
-OUT_PIECES = 4
+SENDS = 13
+(
+    UP, DOWN, ACROSS, RELAY, RATE, FIRST, CON, OUT, IN_RING, CON_RING, OUT_RING, SIBLING, SUMS,
+) = range(SENDS)
+OUT_PIECES = 8
 
 
 def layer_kernel(
     n_sp, n_fs, tok, wq, wf, wv, cg, cm, ci, ro, co, rate, init, headroom, gain, taps, bias,
     out, tokens, win, wcon, wout, rates, first_state, state, ext, both, sib_send, sib_recv, mine,
-    z_send, z_recv, rl_recv, stage_in, stage_con, stage_out, loc_in, loc_con, loc_out, loc_sem,
-    send_sem, in_send, win_z, wcon_z, wout_z, win_f, late_f, tok_z, tok_t, rate_z, ring_send, late_send,
-    down_send, own_send, tok_t_send, sib_sem, sib_out, zr_sem, rl_sem, rs_send,
+    z_send, z_recv, rl_recv, stage_in, stage_con, stage_out, loc_in, loc_sem, out_sem, win_z,
+    wcon_z, wout_z, in_f, con_f, out_f, end_f, tok_z, tok_t, sib_sem, zr_sem, rl_sem,
 ):
     sp, fs, tp = lax.axis_index("sp"), lax.axis_index("fs"), lax.axis_index("tp")
     other = 1 - tp
@@ -245,13 +248,13 @@
 
     def stage(z, in_to, con_to, out_to, place):
         copies = []
-        for some, to, sem in ((rec_parts, in_to, loc_in), (con_parts, con_to, loc_con)):
+        for some, to, sem in ((rec_parts, in_to, loc_in.at[place]), (con_parts, con_to, loc_sem.at[0])):
             for ref, at, width in some:
                 src = ref.at[:, pl.ds(pl.multiple_of(z * width, width), width)]
-                copies.append((src, to.at[:, pl.ds(at, width)], sem.at[place]))
+                copies.append((src, to.at[:, pl.ds(at, width)], sem))
         for ref, at, width in ((ro, 0, rec), (co, rec, con)):
             src = ref.at[pl.ds(pl.multiple_of(z * width, width), width)]
-            copies.append((src, out_to.at[pl.ds(at, width)], loc_out.at[place]))
+            copies.append((src, out_to.at[pl.ds(at, width)], loc_sem.at[1]))
         return [pltpu.make_async_copy(*copy) for copy in copies]
 
     below, above = sp, n_sp - 1 - sp
@@ -277,7 +280,7 @@
         (tok, tokens.at[sp * 2 + tp]), (rate, rates.at[sp]),
         (init.at[pl.ds(sp * heads, heads)], first_state),
     ]
-    others = [pltpu.make_async_copy(*pair, loc_sem.at[i]) for i, pair in enumerate(others)]
+    others = [pltpu.make_async_copy(*pair, loc_sem.at[2 + i]) for i, pair in enumerate(others)]
     for copy in local + others:
         copy.start()
 
@@ -289,20 +292,16 @@
     pl.semaphore_signal(barrier, inc=1, device_id=sibling, device_id_type=MESH)
     pl.semaphore_wait(barrier, n_sp + 2)
 
-    sent = []
-
     def remote(src, dst, send, recv, to):
         return pltpu.make_async_remote_copy(
             src_ref=src, dst_ref=dst, send_sem=send, recv_sem=recv, device_id=to, device_id_type=MESH,
         )
 
-    def push(src, dst, recv, to):
-        copy = remote(src, dst, send_sem.at[len(sent)], recv, to)
-        copy.start()
-        sent.append(copy)
-
     def arrived(ref, recv):
-        remote(ref, ref, send_sem.at[0], recv, sibling).wait_recv()
+        remote(ref, ref, recv, recv, sibling).wait_recv()
+
+    def gone(ref, i):
+        remote(ref, ref, out_sem.at[i], out_sem.at[i], sibling).wait_send()
 
     def tok_piece(ref, c):
         return ref.at[pl.ds(c * sub, sub)]
@@ -312,43 +311,45 @@
 
     def own_tokens(send, to):
         return [
-            remote(tok_piece(tok, c), token_slot(sp, tp, c), send.at[c], tok_z.at[sp, c], to)
+            remote(tok_piece(tok, c), token_slot(sp, tp, c), send, tok_z.at[sp, c], to)
             for c in range(TOKEN_PIECES)
         ]
 
     def own_up():
-        return own_tokens(own_send.at[0], peer(sp=sp + 1))
+        return own_tokens(out_sem.at[UP], peer(sp=sp + 1))
 
     def own_down():
-        return own_tokens(own_send.at[1], peer(sp=sp - 1))
+        return own_tokens(out_sem.at[DOWN], peer(sp=sp - 1))
 
     def to_sibling(s, c, src=None):
         slot = token_slot(s, tp, c)
-        return remote(slot if src is None else src, slot, tok_t_send.at[s, c], tok_t.at[s, c], sibling)
-
-    def relayed(s, c, send, to):
+        return remote(slot if src is None else src, slot, out_sem.at[ACROSS], tok_t.at[s], sibling)
+
+    def relayed(s, c, to):
         slot = token_slot(s, tp, c)
-        return remote(slot, slot, send.at[s, c], tok_z.at[s, c], to)
+        return remote(slot, slot, out_sem.at[RELAY], tok_z.at[s, c], to)
 
     def start_all(copies):
         for copy in copies:
             copy.start()
 
     def send_in(j):
-        z = to_send(j)
-        push(rate, rates.at[sp], rate_z.at[sp], peer(sp=z))
+        to = peer(sp=to_send(j))
         arrived(stage_in.at[j], loc_in.at[j])
-        push(stage_in.at[j], in_rows(sp, fs, 0, rows), win_z.at[sp], peer(sp=z))
+        remote(rate, rates.at[sp], out_sem.at[RATE], end_f.at[3], to).start()
+        remote(
+            stage_in.at[j], in_rows(sp, fs, 0, rows), out_sem.at[FIRST], win_z.at[sp], to
+        ).start()
 
     def late_copies():
         copies = []
         for j in range(1, n_sp):
             to = peer(sp=to_send(j))
             copies.append(
-                remote(stage_con.at[j], con_rows(sp, fs), late_send.at[0, j], wcon_z.at[sp], to)
+                remote(stage_con.at[j], con_rows(sp, fs), out_sem.at[CON], wcon_z.at[sp], to)
             )
             copies.append(
-                remote(stage_out.at[j], out_slot(sp, fs), late_send.at[1, j], wout_z.at[sp], to)
+                remote(stage_out.at[j], out_slot(sp, fs), out_sem.at[OUT], wout_z.at[sp], to)
             )
         return copies
 
@@ -357,9 +358,8 @@
 
     for j in range(2, n_sp):
         send_in(j)
-    for j in range(n_sp):
-        arrived(stage_con.at[j] if j else con_rows(sp, fs), loc_con.at[j])
-        arrived(stage_out.at[j] if j else out_slot(sp, fs), loc_out.at[j])
+    arrived(stage_con, loc_sem.at[0])
+    arrived(stage_out, loc_sem.at[1])
     start_all(late_copies()[:2])
     for copy in others:
         copy.wait()
@@ -380,7 +380,6 @@
     def z_in(j):
         z = near(j)
         arrived(in_rows(z, fs, 0, rows), win_z.at[z])
-        arrived(rates.at[z], rate_z.at[z])
 
     def z_late(j):
         z = near(j)
@@ -394,13 +393,11 @@
         s, half = place(k), rows // 2
         whole = in_rows(s, fs, 0, rows)
         copies = (
-            (whole, right), (whole, left), (in_rows(s, left, 0, half), right),
-            (in_rows(s, right, half, half), left),
+            (whole, in_f.at[0, k], right), (whole, in_f.at[1, k], left),
+            (in_rows(s, left, 0, half), end_f.at[0], right),
+            (in_rows(s, right, half, half), end_f.at[0], left),
         )
-        return [
-            remote(piece, piece, in_send.at[i, k], win_f.at[i, k], peer(fs=to))
-            for i, (piece, to) in enumerate(copies)
-        ]
+        return [remote(ref, ref, out_sem.at[IN_RING], sem, peer(fs=to)) for ref, sem, to in copies]
 
     def ring_in(k):
         start_all(in_ring(k)[:2])
@@ -408,28 +405,24 @@
     def ring_in_on(k):
         s = place(k)
         on = in_ring(k)[2:]
-        arrived(in_rows(s, left, 0, rows), win_f.at[0, k])
+        arrived(in_rows(s, left, 0, rows), in_f.at[0, k])
         on[0].start()
-        arrived(in_rows(s, right, 0, rows), win_f.at[1, k])
+        arrived(in_rows(s, right, 0, rows), in_f.at[1, k])
         on[1].start()
 
-    def ring_in_end(k):
-        s, half = place(k), rows // 2
-        arrived(in_rows(s, across, 0, half), win_f.at[2, k])
-        arrived(in_rows(s, across, half, half), win_f.at[3, k])
+    def ring_in_end():
+        arrived(win.at[pl.ds(0, n_sp * rows)], end_f.at[0])
 
     def late_ring(k):
         s = place(k)
-        mine_con, mine_out = con_rows(s, fs), out_slot(s, fs)
-        passed_con, passed_out = con_rows(s, left), out_slot(s, right)
+        own_con, own_out = con_rows(s, fs), out_slot(s, fs)
         copies = (
-            (mine_con, right), (mine_out, left), (mine_con, left), (mine_out, right),
-            (passed_con, right), (passed_out, left),
+            (own_con, CON_RING, con_f.at[k], right), (own_out, OUT_RING, out_f.at[k], left),
+            (own_con, CON_RING, end_f.at[1], left), (own_out, OUT_RING, end_f.at[2], right),
+            (con_rows(s, left), CON_RING, end_f.at[1], right),
+            (out_slot(s, right), OUT_RING, end_f.at[2], left),
         )
-        return [
-            remote(piece, piece, ring_send.at[i, k], late_f.at[i, k], peer(fs=to))
-            for i, (piece, to) in enumerate(copies)
-        ]
+        return [remote(ref, ref, out_sem.at[i], sem, peer(fs=to)) for ref, i, sem, to in copies]
 
     def ring_late(k):
         start_all(late_ring(k)[:4])
@@ -437,22 +430,19 @@
     def ring_late_on(k):
         s = place(k)
         on = late_ring(k)[4:]
-        arrived(con_rows(s, left), late_f.at[0, k])
+        arrived(con_rows(s, left), con_f.at[k])
         on[0].start()
-        arrived(out_slot(s, right), late_f.at[1, k])
+        arrived(out_slot(s, right), out_f.at[k])
         on[1].start()
 
-    def ring_late_end(k):
-        s = place(k)
-        arrived(con_rows(s, right), late_f.at[2, k])
-        arrived(out_slot(s, left), late_f.at[3, k])
-        arrived(con_rows(s, across), late_f.at[4, k])
-        arrived(out_slot(s, across), late_f.at[5, k])
+    def ring_late_end():
+        arrived(wcon.at[pl.ds(0, 2 * n_sp * rows)], end_f.at[1])
+        arrived(wout.at[pl.ds(0, 2 * n_sp)], end_f.at[2])
 
     def relay(s, c, step_by):
         arrived(token_slot(s, tp, c), tok_z.at[s, c])
         if step_by:
-            relayed(s, c, down_send, peer(sp=sp + step_by)).start()
+            relayed(s, c, peer(sp=sp + step_by)).start()
         to_sibling(s, c).start()
 
     def relays(when, s, step_by, pieces=range(TOKEN_PIECES)):
@@ -517,12 +507,14 @@
         start_all(own_up())
 
     ring_late_on(1)
+    relays(sp == 0, 1, 0)
+    relays(sp == top, top - 1, 0)
     z_late(2)
     ring_late(2)
     z_late(3)
     ring_late(3)
-    for k in range(n_sp):
-        ring_in_end(k)
+    ring_in_end()
+    arrived(rates.at[pl.ds(0, n_sp - 1)], end_f.at[3])
 
     for h in range(heads):
         state[h] = first_state[h].T
@@ -537,13 +529,14 @@
     length = 2 * span
 
     def sib_copy(s, c):
-        return remote(sib_send.at[s, c], sib_recv.at[s, c], sib_out.at[s, c], sib_sem.at[s, c], sibling)
+        return remote(sib_send.at[s, c], sib_recv.at[s, c], out_sem.at[SIBLING], sib_sem.at[s, c], sibling)
 
     def z_copy(s, c):
-        return remote(z_send.at[s, c], z_recv.at[sp, c], rs_send.at[s, c], zr_sem.at[sp, c], peer(sp=s))
+        return remote(z_send.at[s, c], z_recv.at[sp, c], out_sem.at[SUMS], zr_sem.at[sp], peer(sp=s))
 
     def edge_copy(s, c, to):
-        return remote(z_send.at[s, c], rl_recv.at[s, c], rs_send.at[s, c], rl_sem.at[s, c], peer(sp=to))
+        landing, sem = rl_recv.at[s % 2, c], rl_sem.at[s % 2, c]
+        return remote(z_send.at[s, c], landing, out_sem.at[SUMS], sem, peer(sp=to))
 
     def through_low(s):
         return jnp.logical_and(sp == 0, s >= 2)
@@ -560,8 +553,8 @@
         edge = jnp.logical_or(through_low(s), through_high(s))
         return jnp.logical_not(jnp.logical_or(jnp.logical_or(edge, joins(s)), s == sp))
 
-    def pass_on(s):
-        for c in range(chunks):
+    def pass_on(s, pieces=range(OUT_PIECES)):
+        for c in pieces:
             sib_copy(s, c).wait_recv()
             total = mine[s, c] + sib_recv[s, c].astype(F32)
             mine[s, c] = total
@@ -584,23 +577,24 @@
 
     def join(s):
         for c in range(chunks):
-            arrived(rl_recv.at[s, c], rl_sem.at[s, c])
-            z_send[s, c] = (mine[s, c] + rl_recv[s, c].astype(F32)).astype(BF16)
+            arrived(rl_recv.at[s % 2, c], rl_sem.at[s % 2, c])
+            z_send[s, c] = (mine[s, c] + rl_recv[s % 2, c].astype(F32)).astype(BF16)
             z_copy(s, c).start()
 
     def project_out(s):
-        for c in range(chunks):
-            columns = jnp.concatenate(
-                [wout[c * shards_in + i] for i in range(shards_in)], axis=1
-            )
-            partial = jnp.dot(
-                both[s], columns, preferred_element_type=F32
-            )
+        wider = 2 * shards_in
+        for n in range(0, n_sp * n_fs, wider):
+            columns = jnp.concatenate([wout[n + i] for i in range(wider)], axis=1)
+            partial = jnp.dot(both[s], columns, preferred_element_type=F32)
             first = partial[:span]
             second = partial[span:]
-            mine[s, c] = jnp.where(tp == 0, first, second)
-            sib_send[s, c] = jnp.where(tp == 0, second, first).astype(BF16)
-            sib_copy(s, c).start()
+            own = jnp.where(tp == 0, first, second)
+            given = jnp.where(tp == 0, second, first).astype(BF16)
+            for i in range(2):
+                c = n // shards_in + i
+                mine[s, c] = own[:, i * chunk : (i + 1) * chunk]
+                sib_send[s, c] = given[:, i * chunk : (i + 1) * chunk]
+                sib_copy(s, c).start()
 
     def convolve(s):
         block = jnp.concatenate([tokens[2 * s], tokens[2 * s + 1]], axis=0)
@@ -614,9 +608,8 @@
         both[s, :, rec:] = (projected[:, :con] * conv).astype(BF16)
 
     def recur(s):
-        relays(jnp.logical_and(edge, s != sp), s, 0)
-        for c in range(TOKEN_PIECES):
-            arrived(token_slot(s, other, c), tok_t.at[s, c])
+        relays(jnp.logical_and(edge, (s - sp) * (s - sp) > 1), s, 0)
+        arrived(tokens.at[2 * s + other], tok_t.at[s])
         block = jnp.concatenate([tokens[2 * s], tokens[2 * s + 1]], axis=0)
 
         def project(at, width):
@@ -675,6 +668,7 @@
         both[s, :, :rec] = jnp.concatenate(halves, axis=0)
 
     lag = jnp.where(sp < 2, 0, 1)
+    first_pieces, last_pieces = range(chunks // 2), range(chunks // 2, chunks)
 
     def step(i, carry):
         s = i - lag
@@ -685,40 +679,47 @@
 
         @pl.when(i == 0)
         def _():
+            relays(high, bottom, 1, early)
             ring_late_on(2)
             relays(low, top - 1, -1)
-            relays(high, bottom, 1)
-            ring_late_on(3)
+            relays(high, bottom, 1, late)
+
+        pl.when(i == 1 - lag)(functools.partial(ring_late_on, 3))
+        relays(jnp.logical_and(i == 1, low), top, -1, early)
+        relays(jnp.logical_and(i == 1, high), 1, 1, early)
 
         @pl.when(i == 1)
         def _():
-            relays(low, top, -1)
-            relays(high, 1, 1)
-            for k in range(n_sp):
-                ring_late_end(k)
-
-        @pl.when(jnp.logical_and(i == 1, lag == 0))
-        def _():
+            ring_late_end()
             convolve(0)
-            project_out(0)
-            pass_on(0)
-
-        @pl.when(jnp.logical_and(i > 0, s < n_sp))
+
+        ready = jnp.logical_and(i > 0, s < n_sp)
+
+        @pl.when(jnp.logical_and(ready, s > 0))
         def _():
             convolve(s)
-            project_out(s)
-
-        @pl.when(jnp.logical_and(jnp.logical_and(i > 0, s < n_sp), jnp.logical_or(s > 1, sp > 0)))
+
+        pl.when(ready)(functools.partial(project_out, s))
+        relays(jnp.logical_and(i == 1, low), top, -1, late)
+        relays(jnp.logical_and(i == 1, high), 1, 1, late)
+
+        @pl.when(ready)
         def _():
-            pass_on(s)
-
+            pass_on(s, first_pieces)
+            pl.when(jnp.logical_not(jnp.logical_and(sp == 0, s == 1)))(
+                functools.partial(pass_on, s, last_pieces)
+            )
+
+        pl.when(jnp.logical_and(i == 3, high))(functools.partial(join, 0))
         return carry
 
     lax.fori_loop(0, n_sp + 1, step, 0)
 
-    @pl.when(sp == 0)
-    def _():
-        pass_on(1)
+    @pl.when(lag == 0)
+    def _():
+        pl.when(sp == 0)(functools.partial(pass_on, 1, last_pieces))
+        project_out(0)
+        pass_on(0)
 
     @pl.when(sp == 1)
     def _():
@@ -727,7 +728,7 @@
 
     @pl.when(sp == n_sp - 2)
     def _():
-        for s in range(n_sp - 2):
+        for s in range(1, n_sp - 2):
             join(s)
 
     for d in range(n_sp):
@@ -739,48 +740,35 @@
 
         @pl.when(comes)
         def _():
+            arrived(z_recv.at[d], zr_sem.at[d])
             for c in range(chunks):
-                arrived(z_recv.at[d, c], zr_sem.at[d, c])
                 mine[sp, c] = mine[sp, c] + z_recv[d, c].astype(F32)
 
     for c in range(chunks):
         out[:, c * chunk : (c + 1) * chunk] = mine[sp, c].astype(BF16)
 
-    for copy in sent + late_copies():
-        copy.wait_send()
-    for k in range(n_sp):
-        for copy in in_ring(k) + late_ring(k):
-            copy.wait_send()
+    gone(rates.at[pl.ds(0, n_sp - 1)], RATE)
+    gone(win.at[pl.ds(0, (n_sp - 1) * rows)], FIRST)
+    gone(wcon.at[pl.ds(0, (n_sp - 1) * rows)], CON)
+    gone(wout.at[pl.ds(0, n_sp - 1)], OUT)
+    gone(win.at[pl.ds(0, 3 * n_sp * rows)], IN_RING)
+    gone(wcon.at[pl.ds(0, 3 * n_sp * rows)], CON_RING)
+    gone(wout.at[pl.ds(0, 3 * n_sp)], OUT_RING)
+    gone(tokens.at[pl.ds(0, n_sp)], ACROSS)
+    gone(sib_send, SIBLING)
+    gone(z_send.at[pl.ds(0, n_sp - 1)], SUMS)
 
     @pl.when(sp < n_sp - 1)
     def _():
-        for copy in own_up():
-            copy.wait_send()
+        gone(tokens.at[0], UP)
 
     @pl.when(sp > 0)
     def _():
-        for copy in own_down():
-            copy.wait_send()
-
-    for s in range(n_sp):
-        for c in range(TOKEN_PIECES):
-            to_sibling(s, c).wait_send()
-            forwarded = jnp.logical_or(
-                jnp.logical_and(sp > s, sp < n_sp - 1), jnp.logical_and(sp < s, sp > 0)
-            )
-
-            @pl.when(forwarded)
-            def _():
-                relayed(s, c, down_send, sibling).wait_send()
-
-        for c in range(chunks):
-            sib_copy(s, c).wait_send()
-
-            @pl.when(sp != s)
-            def _():
-                remote(
-                    z_send.at[s, c], rl_recv.at[s, c], rs_send.at[s, c], rl_sem.at[s, c], sibling
-                ).wait_send()
+        gone(tokens.at[0], DOWN)
+
+    @pl.when(inner)
+    def _():
+        gone(tokens.at[pl.ds(0, n_sp - 1)], RELAY)
 
 
 def sequence_shards(n_sp, n_fs, *arrays):
@@ -813,34 +801,25 @@
             pltpu.VMEM(flat, F32),
             pltpu.VMEM(flat, BF16),
             pltpu.VMEM(flat, BF16),
-            pltpu.VMEM(flat, BF16),
+            pltpu.VMEM((2,) + flat[1:], BF16),
             pltpu.VMEM((n_sp, wide // (n_sp * n_fs), 3 * rec), BF16),
             pltpu.VMEM((n_sp, wide // (n_sp * n_fs), 3 * con), BF16),
             pltpu.VMEM((n_sp, rec + con, wide // (n_sp * n_fs)), BF16),
             dma((n_sp,)),
-            dma((n_sp,)),
-            dma((n_sp,)),
-            dma((3,)),
-            dma(((n_sp - 1) * 2,)),
-            dma((4, n_sp)),
+            dma((5,)),
+            dma((SENDS,)),
             dma((n_sp,)),
             dma((n_sp,)),
             dma((n_sp,)),
-            dma((4, n_sp)),
-            dma((6, n_sp)),
-            dma((n_sp, TOKEN_PIECES)),
+            dma((2, n_sp)),
+            dma((n_sp,)),
+            dma((n_sp,)),
+            dma((4,)),
             dma((n_sp, TOKEN_PIECES)),
             dma((n_sp,)),
-            dma((6, n_sp)),
-            dma((2, n_sp)),
-            dma((n_sp, TOKEN_PIECES)),
-            dma((2, TOKEN_PIECES)),
-            dma((n_sp, TOKEN_PIECES)),
             dma((n_sp, OUT_PIECES)),
-            dma((n_sp, OUT_PIECES)),
-            dma((n_sp, OUT_PIECES)),
-            dma((n_sp, OUT_PIECES)),
-            dma((n_sp, OUT_PIECES)),
+            dma((n_sp,)),
+            dma((2, OUT_PIECES)),
         ],
         compiler_params=pltpu.CompilerParams(
             collective_id=0, has_side_effects=True, vmem_limit_bytes=60 * 2**20

time: 113 us -> 108 us (0.956)
  the two profiles are of different devices: /device:TPU:0 before, /device:TPU:28 now
where the time goes in v3:
time: 108 us
  Pallas kernels  106 us (98%)
  local copies, waits for them, and re-layouts  1.88 us (2%)
    pallas_call x1, Pallas kernels, sequence_shards(): pl.pallas_call(functools.partial(layer_kernel, n_sp, n_fs), out_shape=jax...  106 us

profile of v3, /device:TPU:28, one launch (start us, length us, event | category | flops | bytes accessed | tf_op | source)
XLA Modules:
  0.0 107.6 jit_solution(16376997157649977042)
XLA Ops:
  0.0 105.7 %shard_map.145 = bf16[128,2048]{1,0:T(8,128)(2,1)} custom-call(bf16[128,2048]{1,0:T(8,128)(2,1)} %bitcast.8, bf16[128,1024]{1,0:T(8,128)(2,1)} %wq.1, bf16[128,1024]{1,0:T(8,128)(2,1)} %wf.1, bf16[128,1024]{1,0:T(8,128)(2,1)} %wv.1, bf16[128,512]{1,0:T(8,128)(2,1)} %cg.1, bf16[128,512]{1,0:T(8,128)(2,1)} %cm.1, bf16[128,512]{1,0:T(8,128)(2,1)} %ci.1, ...), custom_call_target="tpu_custom_call" | custom-call | tf_op jit(solution)/shard_map/pallas_call | solution.py:784
  105.7 1.9 %copy.17 = bf16[1,128,2048]{2,1,0:T(8,128)(2,1)} copy(bf16[1,128,2048]{2,1,0:T(8,128)(2,1)} %bitcast.7) | data formatting | bytes 1048576

commit v4 on v3

--- a/solution.py
+++ b/solution.py
@@ -205,7 +205,7 @@
     n_sp, n_fs, tok, wq, wf, wv, cg, cm, ci, ro, co, rate, init, headroom, gain, taps, bias,
     out, tokens, win, wcon, wout, rates, first_state, state, ext, both, sib_send, sib_recv, mine,
     z_send, z_recv, rl_recv, stage_in, stage_con, stage_out, loc_in, loc_sem, out_sem, win_z,
-    wcon_z, wout_z, in_f, con_f, out_f, end_f, tok_z, tok_t, sib_sem, zr_sem, rl_sem,
+    wcon_z, wout_z, in_f, con_f, out_f, out_end, end_f, tok_z, tok_t, sib_sem, zr_sem, rl_sem,
 ):
     sp, fs, tp = lax.axis_index("sp"), lax.axis_index("fs"), lax.axis_index("tp")
     other = 1 - tp
@@ -234,6 +234,7 @@
     across = ring(lax.rem(at_ring + 2, n_fs))
     sibling = peer(tp=other)
 
+    depth = rec + con
     rec_parts = [(ref, i * rec, rec) for i, ref in enumerate((wq, wf, wv))]
     con_parts = [(ref, i * con, con) for i, ref in enumerate((cg, cm, ci))]
 
@@ -336,22 +337,28 @@
     def send_in(j):
         to = peer(sp=to_send(j))
         arrived(stage_in.at[j], loc_in.at[j])
-        remote(rate, rates.at[sp], out_sem.at[RATE], end_f.at[3], to).start()
+        remote(rate, rates.at[sp], out_sem.at[RATE], end_f.at[2], to).start()
         remote(
             stage_in.at[j], in_rows(sp, fs, 0, rows), out_sem.at[FIRST], win_z.at[sp], to
         ).start()
 
-    def late_copies():
-        copies = []
-        for j in range(1, n_sp):
-            to = peer(sp=to_send(j))
-            copies.append(
-                remote(stage_con.at[j], con_rows(sp, fs), out_sem.at[CON], wcon_z.at[sp], to)
+    def con_copies():
+        return [
+            remote(
+                stage_con.at[j], con_rows(sp, fs), out_sem.at[CON], wcon_z.at[sp],
+                peer(sp=to_send(j)),
             )
-            copies.append(
-                remote(stage_out.at[j], out_slot(sp, fs), out_sem.at[OUT], wout_z.at[sp], to)
+            for j in range(1, n_sp)
+        ]
+
+    def out_copies():
+        return [
+            remote(
+                stage_out.at[j], out_slot(sp, fs), out_sem.at[OUT], wout_z.at[sp],
+                peer(sp=to_send(j)),
             )
-        return copies
+            for j in range(1, n_sp)
+        ]
 
     low, high = sp == 1, sp == n_sp - 2
     send_in(1)
@@ -360,7 +367,7 @@
         send_in(j)
     arrived(stage_con, loc_sem.at[0])
     arrived(stage_out, loc_sem.at[1])
-    start_all(late_copies()[:2])
+    start_all(con_copies()[:1])
     for copy in others:
         copy.wait()
 
@@ -372,6 +379,7 @@
     def _():
         start_all(own_down())
 
+    start_all(out_copies()[:1])
     for c in range(TOKEN_PIECES):
         to_sibling(sp, c, tok_piece(tok, c)).start()
 
@@ -381,63 +389,72 @@
         z = near(j)
         arrived(in_rows(z, fs, 0, rows), win_z.at[z])
 
-    def z_late(j):
+    def z_con(j):
         z = near(j)
         arrived(con_rows(z, fs), wcon_z.at[z])
+
+    def z_out(j):
+        z = near(j)
         arrived(out_slot(z, fs), wout_z.at[z])
 
     def place(j):
         return near(j) if j else sp
 
+    def ring_of(k, whole, part, sem, landed, last):
+        s = place(k)
+        copies = (
+            (whole(s, fs), landed.at[0, k], right), (whole(s, fs), landed.at[1, k], left),
+            (part(s, left, 0), last, right), (part(s, right, 1), last, left),
+        )
+        return [remote(ref, ref, out_sem.at[sem], to_sem, peer(fs=to)) for ref, to_sem, to in copies]
+
+    def pass_ring(k, whole, landed, copies):
+        s = place(k)
+        arrived(whole(s, left), landed.at[0, k])
+        copies[2].start()
+        arrived(whole(s, right), landed.at[1, k])
+        copies[3].start()
+
+    def in_whole(s, f):
+        return in_rows(s, f, 0, rows)
+
     def in_ring(k):
-        s, half = place(k), rows // 2
-        whole = in_rows(s, fs, 0, rows)
-        copies = (
-            (whole, in_f.at[0, k], right), (whole, in_f.at[1, k], left),
-            (in_rows(s, left, 0, half), end_f.at[0], right),
-            (in_rows(s, right, half, half), end_f.at[0], left),
+        half = rows // 2
+        return ring_of(
+            k, in_whole, lambda s, f, h: in_rows(s, f, h * half, half), IN_RING, in_f, end_f.at[0]
         )
-        return [remote(ref, ref, out_sem.at[IN_RING], sem, peer(fs=to)) for ref, sem, to in copies]
+
+    def con_ring(k):
+        half = rows // 2
+        return ring_of(
+            k, con_rows, lambda s, f, h: con_rows(s, f).at[pl.ds(h * half, half)], CON_RING, con_f,
+            end_f.at[1],
+        )
+
+    def out_ring(k):
+        half = depth // 2
+        return ring_of(
+            k, out_slot, lambda s, f, h: out_slot(s, f).at[pl.ds(h * half, half)], OUT_RING, out_f,
+            out_end.at[k],
+        )
 
     def ring_in(k):
         start_all(in_ring(k)[:2])
 
     def ring_in_on(k):
-        s = place(k)
-        on = in_ring(k)[2:]
-        arrived(in_rows(s, left, 0, rows), in_f.at[0, k])
-        on[0].start()
-        arrived(in_rows(s, right, 0, rows), in_f.at[1, k])
-        on[1].start()
-
-    def ring_in_end():
-        arrived(win.at[pl.ds(0, n_sp * rows)], end_f.at[0])
-
-    def late_ring(k):
-        s = place(k)
-        own_con, own_out = con_rows(s, fs), out_slot(s, fs)
-        copies = (
-            (own_con, CON_RING, con_f.at[k], right), (own_out, OUT_RING, out_f.at[k], left),
-            (own_con, CON_RING, end_f.at[1], left), (own_out, OUT_RING, end_f.at[2], right),
-            (con_rows(s, left), CON_RING, end_f.at[1], right),
-            (out_slot(s, right), OUT_RING, end_f.at[2], left),
-        )
-        return [remote(ref, ref, out_sem.at[i], sem, peer(fs=to)) for ref, i, sem, to in copies]
-
-    def ring_late(k):
-        start_all(late_ring(k)[:4])
-
-    def ring_late_on(k):
-        s = place(k)
-        on = late_ring(k)[4:]
-        arrived(con_rows(s, left), con_f.at[k])
-        on[0].start()
-        arrived(out_slot(s, right), out_f.at[k])
-        on[1].start()
-
-    def ring_late_end():
-        arrived(wcon.at[pl.ds(0, 2 * n_sp * rows)], end_f.at[1])
-        arrived(wout.at[pl.ds(0, 2 * n_sp)], end_f.at[2])
+        pass_ring(k, in_whole, in_f, in_ring(k))
+
+    def ring_con(k):
+        start_all(con_ring(k)[:2])
+
+    def ring_con_on(k):
+        pass_ring(k, con_rows, con_f, con_ring(k))
+
+    def ring_out(k):
+        start_all(out_ring(k)[:2])
+
+    def ring_out_on(k):
+        pass_ring(k, out_slot, out_f, out_ring(k))
 
     def relay(s, c, step_by):
         arrived(token_slot(s, tp, c), tok_z.at[s, c])
@@ -458,9 +475,9 @@
         z_in(2)
         ring_in(2)
 
-    def first_late():
-        z_late(1)
-        ring_late(1)
+    def first_con():
+        z_con(1)
+        ring_con(1)
 
     inner = jnp.logical_not(edge)
     ring_in(0)
@@ -468,7 +485,7 @@
     ring_in(1)
     pl.when(inner)(second_in)
     ring_in_on(0)
-    ring_late(0)
+    ring_con(0)
 
     @pl.when(low)
     def _():
@@ -482,39 +499,63 @@
 
     @pl.when(edge)
     def _():
-        first_late()
+        first_con()
         second_in()
 
     z_in(3)
     ring_in(3)
-    start_all(late_copies()[2:])
+    start_all(con_copies()[1:])
 
     @pl.when(high)
     def _():
         start_all(own_down())
-
-    pl.when(inner)(first_late)
+        start_all(out_copies()[1:])
+
+    pl.when(inner)(first_con)
     ring_in_on(2)
     relays(low, bottom, 1, early)
     relays(high, top, -1, early)
-    ring_in_on(3)
-    ring_late_on(0)
     relays(low, bottom, 1, late)
     relays(high, top, -1, late)
 
+    @pl.when(jnp.logical_not(high))
+    def _():
+        start_all(out_copies()[1:])
+
     @pl.when(low)
     def _():
         start_all(own_up())
 
-    ring_late_on(1)
+    ring_in_on(3)
+    ring_con_on(0)
+    ring_con_on(1)
     relays(sp == 0, 1, 0)
     relays(sp == top, top - 1, 0)
-    z_late(2)
-    ring_late(2)
-    z_late(3)
-    ring_late(3)
-    ring_in_end()
-    arrived(rates.at[pl.ds(0, n_sp - 1)], end_f.at[3])
+    z_con(2)
+    ring_con(2)
+    z_con(3)
+    ring_con(3)
+    ring_out(0)
+    z_out(1)
+    ring_out(1)
+    relays(low, top - 1, -1)
+    relays(high, bottom, 1)
+    ring_con_on(2)
+    ring_con_on(3)
+
+    late_start = sp < 2
+    start = jnp.where(late_start, 1, 0)
+
+    def near_out_on():
+        ring_out_on(0)
+        ring_out_on(1)
+        for k in (2, 3):
+            z_out(k)
+            ring_out(k)
+
+    pl.when(jnp.logical_not(late_start))(near_out_on)
+    arrived(win.at[pl.ds(0, n_sp * rows)], end_f.at[0])
+    arrived(rates.at[pl.ds(0, n_sp - 1)], end_f.at[2])
 
     for h in range(heads):
         state[h] = first_state[h].T
@@ -531,11 +572,18 @@
     def sib_copy(s, c):
         return remote(sib_send.at[s, c], sib_recv.at[s, c], out_sem.at[SIBLING], sib_sem.at[s, c], sibling)
 
-    def z_copy(s, c):
-        return remote(z_send.at[s, c], z_recv.at[sp, c], out_sem.at[SUMS], zr_sem.at[sp], peer(sp=s))
+    def final_copy(s, c, to):
+        return remote(
+            z_send.at[s, c], z_recv.at[sp, c], out_sem.at[SUMS], zr_sem.at[sp], peer(sp=to)
+        )
+
+    def joint_copy(s, c, to):
+        landing, sem = rl_recv.at[2, c], rl_sem.at[2, c]
+        return remote(z_send.at[s, c], landing, out_sem.at[SUMS], sem, peer(sp=to))
 
     def edge_copy(s, c, to):
-        landing, sem = rl_recv.at[s % 2, c], rl_sem.at[s % 2, c]
+        t = lax.rem(s, 2)
+        landing, sem = rl_recv.at[t, c], rl_sem.at[t, c]
         return remote(z_send.at[s, c], landing, out_sem.at[SUMS], sem, peer(sp=to))
 
     def through_low(s):
@@ -544,28 +592,32 @@
     def through_high(s):
         return jnp.logical_and(sp == n_sp - 1, s <= n_sp - 3)
 
-    def joins(s):
+    def plain(s):
         return jnp.logical_or(
-            jnp.logical_and(sp == 1, s >= 2), jnp.logical_and(sp == n_sp - 2, s <= n_sp - 3)
+            jnp.logical_and(sp == 0, s == 1), jnp.logical_and(sp == top, s == top - 1)
         )
 
-    def plain(s):
-        edge = jnp.logical_or(through_low(s), through_high(s))
-        return jnp.logical_not(jnp.logical_or(jnp.logical_or(edge, joins(s)), s == sp))
-
-    def pass_on(s, pieces=range(OUT_PIECES)):
-        for c in pieces:
+    per_slot = n_fs // shards_in
+
+    def pieces_of(slots):
+        return [slot * per_slot + i for slot in slots for i in range(per_slot)]
+
+    def own_slots(h):
+        return [place(2 * h), place(2 * h + 1)]
+
+    def pass_on(s, h):
+        for c in pieces_of(own_slots(h)):
             sib_copy(s, c).wait_recv()
             total = mine[s, c] + sib_recv[s, c].astype(F32)
             mine[s, c] = total
 
-            @pl.when(jnp.logical_not(jnp.logical_or(joins(s), s == sp)))
+            @pl.when(jnp.logical_and(edge, s != sp))
             def _():
                 z_send[s, c] = total.astype(BF16)
 
             @pl.when(plain(s))
             def _():
-                z_copy(s, c).start()
+                final_copy(s, c, s).start()
 
             @pl.when(through_low(s))
             def _():
@@ -575,23 +627,31 @@
             def _():
                 edge_copy(s, c, n_sp - 2).start()
 
-    def join(s):
-        for c in range(chunks):
-            arrived(rl_recv.at[s % 2, c], rl_sem.at[s % 2, c])
-            z_send[s, c] = (mine[s, c] + rl_recv[s % 2, c].astype(F32)).astype(BF16)
-            z_copy(s, c).start()
-
-    def project_out(s):
-        wider = 2 * shards_in
-        for n in range(0, n_sp * n_fs, wider):
-            columns = jnp.concatenate([wout[n + i] for i in range(wider)], axis=1)
+    def join(t, h):
+        s = jnp.where(low, (2, 3, 0)[t], (0, 1, 3)[t])
+        to = jnp.where(low, (2, 2, 0)[t], (1, 1, 3)[t])
+        rising = low if t < 2 else high
+        slots = [jnp.where(rising, 2 * h + i, n_sp - 1 - 2 * h - i) for i in range(2)]
+        on = (high, low, None)[t]
+        for c in pieces_of(slots):
+            arrived(rl_recv.at[t, c], rl_sem.at[t, c])
+            z_send[s, c] = (mine[s, c] + rl_recv[t, c].astype(F32)).astype(BF16)
+            if on is None:
+                final_copy(s, c, to).start()
+            else:
+                pl.when(on)(joint_copy(s, c, to).start)
+                pl.when(jnp.logical_not(on))(final_copy(s, c, to).start)
+
+    def project_out(s, h):
+        for slot in own_slots(h):
+            columns = jnp.concatenate([wout[slot * n_fs + i] for i in range(n_fs)], axis=1)
             partial = jnp.dot(both[s], columns, preferred_element_type=F32)
             first = partial[:span]
             second = partial[span:]
             own = jnp.where(tp == 0, first, second)
             given = jnp.where(tp == 0, second, first).astype(BF16)
-            for i in range(2):
-                c = n // shards_in + i
+            for i in range(per_slot):
+                c = slot * per_slot + i
                 mine[s, c] = own[:, i * chunk : (i + 1) * chunk]
                 sib_send[s, c] = given[:, i * chunk : (i + 1) * chunk]
                 sib_copy(s, c).start()
@@ -667,76 +727,78 @@
             halves.append(jnp.concatenate(pieces, axis=1))
         both[s, :, :rec] = jnp.concatenate(halves, axis=0)
 
-    lag = jnp.where(sp < 2, 0, 1)
-    first_pieces, last_pieces = range(chunks // 2), range(chunks // 2, chunks)
-
-    def step(i, carry):
-        s = i - lag
-
-        @pl.when(jnp.logical_and(s >= 0, s < n_sp))
+    def out_end_of(h):
+        for k in (2 * h, 2 * h + 1):
+            arrived(out_slot(place(k), across), out_end.at[k])
+
+    def give(s, *halves):
+        for h in halves:
+            project_out(s, h)
+        for h in halves:
+            pass_on(s, h)
+
+    def step(s, carry):
+        recur(s)
+        pl.when(jnp.logical_and(s == 0, late_start))(near_out_on)
+
+        @pl.when(s == 2 * start)
         def _():
-            recur(s)
-
-        @pl.when(i == 0)
+            ring_out_on(2)
+            ring_out_on(3)
+
+        relays(jnp.logical_and(s == 0, high), 1, 1)
+        relays(jnp.logical_and(s == 1, low), top, -1, early)
+        relays(jnp.logical_and(s == 2, low), top, -1, late)
+
+        @pl.when(s == start)
         def _():
-            relays(high, bottom, 1, early)
-            ring_late_on(2)
-            relays(low, top - 1, -1)
-            relays(high, bottom, 1, late)
-
-        pl.when(i == 1 - lag)(functools.partial(ring_late_on, 3))
-        relays(jnp.logical_and(i == 1, low), top, -1, early)
-        relays(jnp.logical_and(i == 1, high), 1, 1, early)
-
-        @pl.when(i == 1)
+            arrived(wcon.at[pl.ds(0, n_sp * rows)], end_f.at[1])
+            pl.when(late_start)(functools.partial(convolve, 0))
+
+        pl.when(s >= start)(functools.partial(convolve, s))
+        pl.when(s == start)(functools.partial(out_end_of, 0))
+        others_rows = jnp.logical_and(s >= start, s != sp)
+        pl.when(others_rows)(functools.partial(give, s, 0))
+
+        pl.when(s == 2 * start)(functools.partial(out_end_of, 1))
+        held = jnp.logical_and(late_start, s == 1)
+        pl.when(jnp.logical_and(others_rows, jnp.logical_not(held)))(functools.partial(give, s, 1))
+
+        @pl.when(jnp.logical_and(s == 1, high))
         def _():
-            ring_late_end()
-            convolve(0)
-
-        ready = jnp.logical_and(i > 0, s < n_sp)
-
-        @pl.when(jnp.logical_and(ready, s > 0))
-        def _():
-            convolve(s)
-
-        pl.when(ready)(functools.partial(project_out, s))
-        relays(jnp.logical_and(i == 1, low), top, -1, late)
-        relays(jnp.logical_and(i == 1, high), 1, 1, late)
-
-        @pl.when(ready)
-        def _():
-            pass_on(s, first_pieces)
-            pl.when(jnp.logical_not(jnp.logical_and(sp == 0, s == 1)))(
-                functools.partial(pass_on, s, last_pieces)
-            )
-
-        pl.when(jnp.logical_and(i == 3, high))(functools.partial(join, 0))
+            join(0, 0)
+            join(0, 1)
+
+        pl.when(jnp.logical_and(s == 2, low))(functools.partial(join, 0, 0))
         return carry
 
-    lax.fori_loop(0, n_sp + 1, step, 0)
-
-    @pl.when(lag == 0)
-    def _():
-        pl.when(sp == 0)(functools.partial(pass_on, 1, last_pieces))
-        project_out(0)
-        pass_on(0)
-
-    @pl.when(sp == 1)
-    def _():
-        for s in range(2, n_sp):
-            join(s)
-
-    @pl.when(sp == n_sp - 2)
-    def _():
-        for s in range(1, n_sp - 2):
-            join(s)
+    lax.fori_loop(0, n_sp, step, 0)
+    @pl.when(sp == 0)
+    def _():
+        give(1, 1)
+        give(0, 0, 1)
+
+    pl.when(low)(functools.partial(give, 0, 0, 1))
+
+    pl.when(low)(functools.partial(join, 0, 1))
+
+    pl.when(sp > 0)(functools.partial(give, sp, 0, 1))
+
+    @pl.when(low)
+    def _():
+        for h in range(2):
+            join(1, h)
+            join(2, h)
+
+    @pl.when(high)
+    def _():
+        for h in range(2):
+            join(1, h)
+        for h in range(2):
+            join(2, h)
 
     for d in range(n_sp):
-        comes = sp != d
-        if d == 0:
-            comes = jnp.logical_and(comes, sp < 2)
-        if d == n_sp - 1:
-            comes = jnp.logical_and(comes, sp > n_sp - 3)
+        comes = (sp - d) * (sp - d) == 1
 
         @pl.when(comes)
         def _():
@@ -783,7 +845,7 @@
     flat = (n_sp, OUT_PIECES, span, chunk)
     mixed = pl.pallas_call(
         functools.partial(layer_kernel, n_sp, n_fs),
-        out_shape=jax.ShapeDtypeStruct((span, wide), BF16),
+        out_shape=pltpu.VMEM((span, wide), BF16),
         in_specs=[hbm] * 11 + [vmem] * 4,
         out_specs=vmem,
         scratch_shapes=[
@@ -801,7 +863,7 @@
             pltpu.VMEM(flat, F32),
             pltpu.VMEM(flat, BF16),
             pltpu.VMEM(flat, BF16),
-            pltpu.VMEM((2,) + flat[1:], BF16),
+            pltpu.VMEM((3,) + flat[1:], BF16),
             pltpu.VMEM((n_sp, wide // (n_sp * n_fs), 3 * rec), BF16),
             pltpu.VMEM((n_sp, wide // (n_sp * n_fs), 3 * con), BF16),
             pltpu.VMEM((n_sp, rec + con, wide // (n_sp * n_fs)), BF16),
@@ -812,14 +874,15 @@
             dma((n_sp,)),
             dma((n_sp,)),
             dma((2, n_sp)),
+            dma((2, n_sp)),
+            dma((2, n_sp)),
             dma((n_sp,)),
-            dma((n_sp,)),
-            dma((4,)),
+            dma((3,)),
             dma((n_sp, TOKEN_PIECES)),
             dma((n_sp,)),
             dma((n_sp, OUT_PIECES)),
             dma((n_sp,)),
-            dma((2, OUT_PIECES)),
+            dma((3, OUT_PIECES)),
         ],
         compiler_params=pltpu.CompilerParams(
             collective_id=0, has_side_effects=True, vmem_limit_bytes=60 * 2**20

time: 108 us -> 104 us (0.963)
  Pallas kernels: 106 us -> 103 us
    pallas_call x1, Pallas kernels: 106 us -> 103 us  [sequence_shards(): pl.pallas_call(functools.partial(layer_kernel, n_sp, n_fs), out_shape=plt...]
    unnamed x1, local copies, waits for them, and re-layouts: 1.88 us -> 0.8 us
where the time goes in v4:
time: 104 us
  Pallas kernels  103 us (99%)
    pallas_call x1, Pallas kernels, sequence_shards(): pl.pallas_call(functools.partial(layer_kernel, n_sp, n_fs), out_shape=plt...  103 us

profile of v4, /device:TPU:28, one launch (start us, length us, event | category | flops | bytes accessed | tf_op | source)
XLA Modules:
  0.0 104.1 jit_solution(13189231632830140350)
XLA Ops:
  0.0 103.3 %shard_map.145 = bf16[128,2048]{1,0:T(8,128)(2,1)S(1)} custom-call(bf16[128,2048]{1,0:T(8,128)(2,1)} %bitcast.8, bf16[128,1024]{1,0:T(8,128)(2,1)} %wq.1, bf16[128,1024]{1,0:T(8,128)(2,1)} %wf.1, bf16[128,1024]{1,0:T(8,128)(2,1)} %wv.1, bf16[128,512]{1,0:T(8,128)(2,1)} %cg.1, bf16[128,512]{1,0:T(8,128)(2,1)} %cm.1, bf16[128,512]{1,0:T(8,128)(2,1)} %ci.1, ...), custom_call_target="tpu_custom_call" | custom-call | tf_op jit(solution)/shard_map/pallas_call | solution.py:846
  103.3 0.8 copy.17

commit v5 on v4

--- a/solution.py
+++ b/solution.py
@@ -668,7 +668,10 @@
         both[s, :, rec:] = (projected[:, :con] * conv).astype(BF16)
 
     def recur(s):
-        relays(jnp.logical_and(edge, (s - sp) * (s - sp) > 1), s, 0)
+        relayed_before = jnp.logical_or(
+            (s - sp) * (s - sp) <= 1, jnp.logical_and(sp == 0, s == 2)
+        )
+        relays(jnp.logical_and(edge, jnp.logical_not(relayed_before)), s, 0)
         arrived(tokens.at[2 * s + other], tok_t.at[s])
         block = jnp.concatenate([tokens[2 * s], tokens[2 * s + 1]], axis=0)
 
@@ -739,6 +742,7 @@
 
     def step(s, carry):
         recur(s)
+        relays(jnp.logical_and(s == 1, sp == 0), 2, 0)
         pl.when(jnp.logical_and(s == 0, late_start))(near_out_on)
 
         @pl.when(s == 2 * start)
@@ -756,6 +760,7 @@
             pl.when(late_start)(functools.partial(convolve, 0))
 
         pl.when(s >= start)(functools.partial(convolve, s))
+        pl.when(jnp.logical_and(s == 3, low))(functools.partial(join, 0, 1))
         pl.when(s == start)(functools.partial(out_end_of, 0))
         others_rows = jnp.logical_and(s >= start, s != sp)
         pl.when(others_rows)(functools.partial(give, s, 0))
@@ -780,7 +785,6 @@
 
     pl.when(low)(functools.partial(give, 0, 0, 1))
 
-    pl.when(low)(functools.partial(join, 0, 1))
 
     pl.when(sp > 0)(functools.partial(give, sp, 0, 1))
 

time: 104 us -> 102 us (0.981)
  Pallas kernels: 103 us -> 101 us
    pallas_call x1, Pallas kernels: 103 us -> 101 us  [sequence_shards(): pl.pallas_call(functools.partial(layer_kernel, n_sp, n_fs), out_shape=plt...]
where the time goes in v5:
time: 102 us
  Pallas kernels  101 us (99%)
    pallas_call x1, Pallas kernels, sequence_shards(): pl.pallas_call(functools.partial(layer_kernel, n_sp, n_fs), out_shape=plt...  101 us

profile of v5, /device:TPU:28, one launch (start us, length us, event | category | flops | bytes accessed | tf_op | source)
XLA Modules:
  0.0 102.1 jit_solution(14040585866156945194)
XLA Ops:
  0.0 101.3 %shard_map.145 = bf16[128,2048]{1,0:T(8,128)(2,1)S(1)} custom-call(bf16[128,2048]{1,0:T(8,128)(2,1)} %bitcast.8, bf16[128,1024]{1,0:T(8,128)(2,1)} %wq.1, bf16[128,1024]{1,0:T(8,128)(2,1)} %wf.1, bf16[128,1024]{1,0:T(8,128)(2,1)} %wv.1, bf16[128,512]{1,0:T(8,128)(2,1)} %cg.1, bf16[128,512]{1,0:T(8,128)(2,1)} %cm.1, bf16[128,512]{1,0:T(8,128)(2,1)} %ci.1, ...), custom_call_target="tpu_custom_call" | custom-call | tf_op jit(solution)/shard_map/pallas_call | solution.py:850
  101.3 0.8 copy.17

commit v6 on v5

--- a/solution.py
+++ b/solution.py
@@ -202,8 +202,8 @@
 
 
 def layer_kernel(
-    n_sp, n_fs, tok, wq, wf, wv, cg, cm, ci, ro, co, rate, init, headroom, gain, taps, bias,
-    out, tokens, win, wcon, wout, rates, first_state, state, ext, both, sib_send, sib_recv, mine,
+    n_sp, n_fs, tok, wq, wf, wv, cg, cm, ci, ro, co, rate, init, headroom_in, gain_in,
+    taps_in, bias_in, out, headroom, gain, taps, bias, tokens, win, wcon, wout, rates, first_state, state, ext, both, sib_send, sib_recv, mine,
     z_send, z_recv, rl_recv, stage_in, stage_con, stage_out, loc_in, loc_sem, out_sem, win_z,
     wcon_z, wout_z, in_f, con_f, out_f, out_end, end_f, tok_z, tok_t, sib_sem, zr_sem, rl_sem,
 ):
@@ -279,7 +279,8 @@
     local += stage(sp, in_rows(sp, fs, 0, rows), con_rows(sp, fs), out_slot(sp, fs), 0)
     others = [
         (tok, tokens.at[sp * 2 + tp]), (rate, rates.at[sp]),
-        (init.at[pl.ds(sp * heads, heads)], first_state),
+        (init.at[pl.ds(sp * heads, heads)], first_state), (headroom_in, headroom), (gain_in, gain),
+        (taps_in, taps), (bias_in, bias),
     ]
     others = [pltpu.make_async_copy(*pair, loc_sem.at[2 + i]) for i, pair in enumerate(others)]
     for copy in local + others:
@@ -745,12 +746,14 @@
         relays(jnp.logical_and(s == 1, sp == 0), 2, 0)
         pl.when(jnp.logical_and(s == 0, late_start))(near_out_on)
 
+        relays(jnp.logical_and(s == 0, high), 1, 1, early)
+
         @pl.when(s == 2 * start)
         def _():
             ring_out_on(2)
             ring_out_on(3)
 
-        relays(jnp.logical_and(s == 0, high), 1, 1)
+        relays(jnp.logical_and(s == 0, high), 1, 1, late)
         relays(jnp.logical_and(s == 1, low), top, -1, early)
         relays(jnp.logical_and(s == 2, low), top, -1, late)
 
@@ -850,9 +853,13 @@
     mixed = pl.pallas_call(
         functools.partial(layer_kernel, n_sp, n_fs),
         out_shape=pltpu.VMEM((span, wide), BF16),
-        in_specs=[hbm] * 11 + [vmem] * 4,
+        in_specs=[hbm] * 15,
         out_specs=vmem,
         scratch_shapes=[
+            pltpu.VMEM((1, headroom.shape[0]), F32),
+            pltpu.VMEM((1, gain.shape[0]), F32),
+            pltpu.VMEM(taps.shape, F32),
+            pltpu.VMEM((1, bias.shape[0]), F32),
             pltpu.VMEM((2 * n_sp, span, wide), BF16),
             pltpu.VMEM((wide, 3 * rec), BF16),
             pltpu.VMEM((wide, 3 * con), BF16),
@@ -872,7 +879,7 @@
             pltpu.VMEM((n_sp, wide // (n_sp * n_fs), 3 * con), BF16),
             pltpu.VMEM((n_sp, rec + con, wide // (n_sp * n_fs)), BF16),
             dma((n_sp,)),
-            dma((5,)),
+            dma((9,)),
             dma((SENDS,)),
             dma((n_sp,)),
             dma((n_sp,)),

time: 102 us -> 102 us (level)
  no operation moved by 1% of the time
where the time goes in v6:
time: 102 us; the launch traced here: 101 us
  Pallas kernels  101 us (99%)
    pallas_call x1, Pallas kernels, sequence_shards(): pl.pallas_call(functools.partial(layer_kernel, n_sp, n_fs), out_shape=plt...  101 us

profile of v6, /device:TPU:28, one launch (start us, length us, event | category | flops | bytes accessed | tf_op | source)
XLA Modules:
  0.0 101.5 jit_solution(15203929758363510962)
XLA Ops:
  0.0 100.6 %shard_map.145 = bf16[128,2048]{1,0:T(8,128)(2,1)S(1)} custom-call(bf16[128,2048]{1,0:T(8,128)(2,1)} %bitcast.8, bf16[128,1024]{1,0:T(8,128)(2,1)} %wq.1, bf16[128,1024]{1,0:T(8,128)(2,1)} %wf.1, bf16[128,1024]{1,0:T(8,128)(2,1)} %wv.1, bf16[128,512]{1,0:T(8,128)(2,1)} %cg.1, bf16[128,512]{1,0:T(8,128)(2,1)} %cm.1, bf16[128,512]{1,0:T(8,128)(2,1)} %ci.1, ...), custom_call_target="tpu_custom_call" | custom-call | tf_op jit(solution)/shard_map/pallas_call | solution.py:853
  100.7 0.8 copy.17
